TPU v7x, 32 devices: a whole 2x2x4 slice. The times are simulated.
32 devices in a mesh: sp: 8 (over z, y), tp: 4 (over x, core).
Axes of the slice: x: 2, y: 2, z: 4, core: 2. Of those that a mesh axis runs over, the one named last changes fastest.
Arguments:
- tokens: bfloat16 [8192, 2048], P('sp'), may hold values from -6 to 6
- in_gain: float32 [2048], replicated, may hold values from 0.1 to 1.9
- w_query: bfloat16 [2048, 1024], P(None, 'tp'), may hold values from -0.125 to 0.125
- w_forget: bfloat16 [2048, 1024], P(None, 'tp'), may hold values from -0.125 to 0.125
- w_input: bfloat16 [2048, 1024], P(None, 'tp'), may hold values from -0.125 to 0.125
- w_outgate: bfloat16 [2048, 1024], P(None, 'tp'), may hold values from -0.125 to 0.125
- w_conv_h: bfloat16 [2048, 1024], P(None, 'tp'), may hold values from -0.125 to 0.125
- w_conv_b: bfloat16 [2048, 1024], P(None, 'tp'), may hold values from -0.125 to 0.125
- w_conv_c: bfloat16 [2048, 1024], P(None, 'tp'), may hold values from -0.125 to 0.125
- forget_floor: float32 [1024], P('tp'), may hold values from 0.84 to 1
- forget_leak: float32 [8192, 1024], P('sp', 'tp'), may hold values from -1 to 0
- state_gain: float32 [128], replicated, may hold values from 0.1 to 1.9
- conv_taps: bfloat16 [3, 1024], P(None, 'tp'), may hold values from -3.5 to 3.5
- group_gain: float32 [128], replicated, may hold values from 0.1 to 1.9
- out_state: bfloat16 [1024, 2048], P('tp'), may hold values from -0.1875 to 0.1875
- out_conv: bfloat16 [1024, 2048], P('tp'), may hold values from -0.1875 to 0.1875
Outputs:
- mixed_out: bfloat16 [8192, 2048], P('sp', 'tp')
All inputs are finite; a program needn't handle non-finite values.
Results may differ from a plain program's by a relative error of at most 0.015.
Values may be sent and summed in bfloat16 or wider, within the bound.
A program may use at most 128 MiB of HBM per device.

v0:
```python
import functools

import jax
import jax.numpy as jnp
from jax import lax
from jax.experimental import pallas as pl
from jax.experimental.pallas import tpu as pltpu
from jax.sharding import PartitionSpec as P

GROUP_FEATURES = 128
CHUNK = 128
ROWS = 256
TAPS = 3
HALO = 8

norm_eps = 1e-06
f32 = jnp.float32
bf16 = jnp.bfloat16


def dot(a, b, dims=((1,), (0,)), precision=None):
    return lax.dot_general(a, b, (dims, ((), ())), precision=precision, preferred_element_type=f32)


def rms(values):
    return values * lax.rsqrt(jnp.mean(values * values, axis=-1, keepdims=True) + norm_eps)


def per_group(values, gain):
    parts = []
    for g in range(values.shape[1] // GROUP_FEATURES):
        parts.append(rms(values[:, g * GROUP_FEATURES : (g + 1) * GROUP_FEATURES]) * gain)
    return jnp.concatenate(parts, axis=1)


def fused_kernel(
    tp, sp,
    tokens, in_gain, wq, wf, wi, wg, wh, wb, wc, floor, leak, state_gain, taps, group_gain,
    out_state, out_conv, result,
    pad, state, offset, read, qdev, gate, conv_all, mix_all, columns, states, logs, sent_state,
    rim, tail, head_conv, head_gate, incoming,
    col_send, col_recv, own_sem, blk_send, fwd_send, blk_recv, st_send, st_recv, log_send, log_recv,
    rim_send, rim_recv,
):
    step, steps = pl.program_id(0), pl.num_programs(0)
    rows = tokens.shape[0]
    me, place = lax.axis_index("tp"), lax.axis_index("sp")
    partner = me + 1 - 2 * lax.rem(me, 2)
    ncols = result.shape[1]
    heads = state.shape[0]
    here = pl.ds(pl.multiple_of(step * rows, rows), rows)
    held = (conv_all, mix_all)

    def col_copy(kind, k):
        target = lax.rem(me + k, tp)
        src = (out_state, out_conv)[kind].at[:, pl.ds(pl.multiple_of(target * ncols, ncols), ncols)]
        dst = columns.at[kind, me]
        if k == 0:
            return pltpu.make_async_copy(src, dst, own_sem.at[kind])
        return pltpu.make_async_remote_copy(
            src, dst, col_send.at[kind, k], col_recv.at[kind, me], device_id={"tp": target}
        )

    def block_copy(kind, t, origin, target, send):
        ref = held[kind].at[origin, t]
        return pltpu.make_async_remote_copy(
            ref, ref, send, blk_recv.at[kind, origin, t], device_id={"tp": target}
        )

    def own_copies(kind, t):
        out = [block_copy(kind, t, me, partner, blk_send.at[kind, 0, t])]
        for k in range(1, tp // 2):
            out.append(block_copy(kind, t, me, lax.rem(me + 2 * k, tp), blk_send.at[kind, k, t]))
        return out

    def relays(kind, t):
        out = []
        for k in range(1, tp // 2):
            origin = lax.rem(me + 2 * k, tp)
            out.append(block_copy(kind, t, origin, partner, fwd_send.at[kind, k, t]))
        return out

    def state_copies(k):
        target = lax.rem(place + k, sp)
        to = {"sp": target}
        return (
            pltpu.make_async_remote_copy(
                sent_state, states.at[place], st_send.at[k], st_recv.at[place], device_id=to
            ),
            pltpu.make_async_remote_copy(
                offset, logs.at[place], log_send.at[k], log_recv.at[place], device_id=to
            ),
        )

    def state_arrivals(k):
        source = lax.rem(place + k, sp)
        to = {"sp": source}
        return (
            pltpu.make_async_remote_copy(
                sent_state, states.at[source], st_send.at[k], st_recv.at[source], device_id=to
            ),
            pltpu.make_async_remote_copy(
                offset, logs.at[source], log_send.at[k], log_recv.at[source], device_id=to
            ),
        )

    rim_copy = pltpu.make_async_remote_copy(
        tail, rim, rim_send.at[0], rim_recv.at[0], device_id={"sp": lax.rem(place + 1, sp)}
    )

    @pl.when(step == 0)
    def _():
        barrier = pltpu.get_barrier_semaphore()
        for k in range(1, tp):
            pl.semaphore_signal(barrier, inc=1, device_id={"tp": lax.rem(me + k, tp)})
        for k in range(1, sp):
            pl.semaphore_signal(barrier, inc=1, device_id={"sp": lax.rem(place + k, sp)})
        pl.semaphore_wait(barrier, tp + sp - 2)
        for kind in (1, 0):
            for k in range(tp):
                col_copy(kind, k).start()
        pad[0:HALO, :] = jnp.zeros((HALO, pad.shape[1]), f32)
        state[...] = jnp.zeros_like(state)
        offset[...] = jnp.zeros_like(offset)

    normed = (rms(tokens[...].astype(f32)) * in_gain[...]).astype(bf16)

    def project(w):
        return dot(normed, w[...]).astype(bf16).astype(f32)

    conv_in = (project(wc) * project(wh)).astype(bf16).astype(f32)
    proj_b = project(wb)
    pad[HALO : HALO + rows, :] = conv_in
    w = taps[...].astype(f32)
    total = w[TAPS - 1 : TAPS] * conv_in
    for j in range(TAPS - 1):
        total += w[j : j + 1] * pad[HALO - (TAPS - 1) + j : HALO - (TAPS - 1) + j + rows, :]
    conv_all[me, step] = per_group(proj_b * total, group_gain[...]).astype(bf16)

    @pl.when(step == 0)
    def _():
        head_conv[...] = conv_in[:HALO]
        head_gate[...] = proj_b[:HALO]

    pad[0:HALO, :] = conv_in[rows - HALO :]

    x = project(wf)
    key = (1.0 - floor[...]) * jax.nn.sigmoid(-x)
    logf = jnp.log(1.0 - key) + leak[...]
    value = dot(normed, wi[...]).astype(bf16)
    query = jax.nn.silu(project(wq))
    gate[here, :] = dot(normed, wg[...]).astype(bf16)

    r = lax.broadcasted_iota(jnp.int32, (CHUNK, CHUNK), 0)
    c = lax.broadcasted_iota(jnp.int32, (CHUNK, CHUNK), 1)
    causal = r >= c
    ones = causal.astype(f32)
    for b in range(rows // CHUNK):
        lo, hi = b * CHUNK, (b + 1) * CHUNK
        at = pl.ds(pl.multiple_of(step * rows + lo, CHUNK), CHUNK)
        cum = dot(ones, logf[lo:hi], precision=lax.Precision.HIGHEST)
        mid = cum[CHUNK // 2 - 1 : CHUNK // 2]
        last = cum[CHUNK - 1 : CHUNK]
        q_mid = query[lo:hi] * jnp.exp(cum - mid)
        k_mid = key[lo:hi] * jnp.exp(mid - cum)
        q_all = q_mid * jnp.exp(mid)
        k_end = (k_mid * jnp.exp(last - mid)).astype(bf16)
        qdev[at, :] = (q_all * jnp.exp(offset[0:1, :])).astype(bf16)
        q_mid, k_mid, q_all = q_mid.astype(bf16), k_mid.astype(bf16), q_all.astype(bf16)
        for h in range(heads):
            s = slice(h * GROUP_FEATURES, (h + 1) * GROUP_FEATURES)
            scores = dot(q_mid[:, s], k_mid[:, s], ((1,), (1,)))
            scores = jnp.where(causal, scores, 0.0).astype(bf16)
            v = value[lo:hi, s]
            old = state[h]
            read[at, s] = dot(scores, v) + dot(q_all[:, s], old.astype(bf16), ((1,), (1,)))
            state[h] = old * jnp.exp(last[:, s]) + dot(v, k_end[:, s], ((0,), (0,)))
        offset[...] += last

    @pl.when(step > 0)
    def _():
        for copy in own_copies(0, step):
            copy.start()

    @pl.when(step == steps - 1)
    def _():
        nb = read.shape[0] // rows
        tail[...] = pad[0:HALO, :]
        sent_state[...] = state[...].astype(bf16)
        rim_copy.start()
        for k in range(1, sp):
            for copy in state_copies(k):
                copy.start()
        rim_copy.wait_recv()
        before = jnp.where(place > 0, rim[...], 0.0)
        ext = jnp.concatenate([before, head_conv[...]], axis=0)
        fixed = w[TAPS - 1 : TAPS] * head_conv[...]
        for j in range(TAPS - 1):
            fixed += w[j : j + 1] * ext[HALO - (TAPS - 1) + j : 2 * HALO - (TAPS - 1) + j]
        fixed = per_group(head_gate[...] * fixed, group_gain[...])
        conv_all[me, 0, 0:HALO, :] = fixed.astype(bf16)

        for k in range(1, sp):
            for copy in state_arrivals(k):
                copy.wait_recv()
        for copy in own_copies(0, 0):
            copy.start()
        incoming[...] = jnp.zeros_like(incoming)

        def hop(p, _):
            decay = jnp.exp(logs[p, 0:1, :])
            for h in range(heads):
                s = slice(h * GROUP_FEATURES, (h + 1) * GROUP_FEATURES)
                incoming[h] = incoming[h] * decay[:, s] + states[p, h].astype(f32)
            return 0

        lax.fori_loop(0, place, hop, 0)

        def merge(t, _):
            at = pl.ds(pl.multiple_of(t * rows, rows), rows)
            for h in range(heads):
                s = slice(h * GROUP_FEATURES, (h + 1) * GROUP_FEATURES)
                whole = read[at, s] + dot(qdev[at, s], incoming[h].astype(bf16), ((1,), (1,)))
                out = rms(whole) * state_gain[...] * jax.nn.silu(gate[at, s].astype(f32))
                mix_all[me, t, :, s] = out.astype(bf16)
            for copy in own_copies(1, t):
                copy.start()
            return 0

        lax.fori_loop(0, nb, merge, 0)

        def relay(kind, t):
            for copy in relays(kind, t):
                copy.wait_recv()
                copy.start()

        def conv_relay(t, _):
            relay(0, t + 1)
            return 0

        lax.fori_loop(0, nb - 1, conv_relay, 0)
        relay(0, 0)
        for kind in range(2):
            col_copy(kind, 0).wait()
            for k in range(1, tp):
                source = lax.rem(me + k, tp)
                ref = columns.at[kind, source]
                pltpu.make_async_remote_copy(
                    ref, ref, col_send.at[kind, k], col_recv.at[kind, source],
                    device_id={"tp": source},
                ).wait_recv()

        def finish(t, _):
            relay(1, t)
            for kind in range(2):
                for k in range(tp // 2):
                    origin = lax.rem(partner + 2 * k, tp)
                    block_copy(kind, t, origin, partner, blk_send.at[kind, 0, t]).wait_recv()
            acc = jnp.zeros((rows, ncols), f32)
            for o in range(tp):
                acc += dot(mix_all[o, t], columns[0, o])
                acc += dot(conv_all[o, t], columns[1, o])
            result[pl.ds(pl.multiple_of(t * rows, rows), rows), :] = acc.astype(bf16)
            return 0

        lax.fori_loop(0, nb, finish, 0)

        def drain(t, _):
            for kind in range(2):
                for copy in own_copies(kind, t) + relays(kind, t):
                    copy.wait_send()
            return 0

        lax.fori_loop(0, nb, drain, 0)
        for kind in range(2):
            for k in range(1, tp):
                col_copy(kind, k).wait_send()
        rim_copy.wait_send()
        for k in range(1, sp):
            for copy in state_copies(k):
                copy.wait_send()


def body(
    tokens, in_gain, w_query, w_forget, w_input, w_outgate, w_conv_h, w_conv_b, w_conv_c,
    forget_floor, forget_leak, state_gain, conv_taps, group_gain, out_state, out_conv,
):
    count, feats = tokens.shape
    width, channels = w_query.shape[1], w_conv_h.shape[1]
    heads = width // GROUP_FEATURES
    tp, sp = lax.axis_size("tp"), lax.axis_size("sp")
    ncols, nb = out_state.shape[1] // tp, count // ROWS

    def whole(*shape):
        return pl.BlockSpec(shape, lambda i: (0,) * len(shape))

    def rows(n):
        return pl.BlockSpec((ROWS, n), lambda i: (i, 0))

    sems = pltpu.SemaphoreType.DMA
    return pl.pallas_call(
        functools.partial(fused_kernel, tp, sp),
        grid=(nb,),
        in_specs=[rows(feats), whole(1, feats)] + [whole(feats, width)] * 4
        + [whole(feats, channels)] * 3
        + [whole(1, width), rows(width), whole(1, GROUP_FEATURES), whole(TAPS, channels),
           whole(1, GROUP_FEATURES)]
        + [pl.BlockSpec(memory_space=pl.ANY)] * 2,
        out_specs=whole(count, ncols),
        out_shape=jax.ShapeDtypeStruct((count, ncols), bf16),
        scratch_shapes=[
            pltpu.VMEM((HALO + ROWS, channels), f32),
            pltpu.VMEM((heads, GROUP_FEATURES, GROUP_FEATURES), f32),
            pltpu.VMEM((HALO, width), f32),
            pltpu.VMEM((count, width), f32),
            pltpu.VMEM((count, width), bf16),
            pltpu.VMEM((count, width), bf16),
            pltpu.VMEM((tp, nb, ROWS, channels), bf16),
            pltpu.VMEM((tp, nb, ROWS, width), bf16),
            pltpu.VMEM((2, tp, width, ncols), bf16),
            pltpu.VMEM((sp, heads, GROUP_FEATURES, GROUP_FEATURES), bf16),
            pltpu.VMEM((sp, HALO, width), f32),
            pltpu.VMEM((heads, GROUP_FEATURES, GROUP_FEATURES), bf16),
            pltpu.VMEM((HALO, channels), f32),
            pltpu.VMEM((HALO, channels), f32),
            pltpu.VMEM((HALO, channels), f32),
            pltpu.VMEM((HALO, channels), f32),
            pltpu.VMEM((heads, GROUP_FEATURES, GROUP_FEATURES), f32),
            sems((2, tp)), sems((2, tp)), sems((2,)),
            sems((2, tp // 2, nb)), sems((2, tp // 2, nb)), sems((2, tp, nb)),
            sems((sp,)), sems((sp,)), sems((sp,)), sems((sp,)), sems((1,)), sems((1,)),
        ],
        compiler_params=pltpu.CompilerParams(
            vmem_limit_bytes=56 * 2**20, collective_id=0, has_side_effects=True
        ),
    )(
        tokens, in_gain[None], w_query, w_forget, w_input, w_outgate, w_conv_h, w_conv_b, w_conv_c,
        forget_floor[None], forget_leak, state_gain[None], conv_taps, group_gain[None],
        out_state, out_conv,
    )


def solution(mesh):
    cols, rows = P(None, "tp"), P("tp", None)
    in_specs = (
        P("sp", None), P(), cols, cols, cols, cols, cols, cols, cols,
        P("tp"), P("sp", "tp"), P(), cols, P(), rows, rows,
    )
    return jax.shard_map(
        body, mesh=mesh, in_specs=in_specs, out_specs=P("sp", "tp"), check_vma=False
    )
```

profile of v0, /device:TPU:1, one launch (start us, length us, event | category | flops | bytes accessed | tf_op | source)
XLA Modules:
  0.0 62.6 jit_solution(18409838214980542585)
XLA Ops:
  0.0 60.3 %shard_map.154 = bf16[1024,512]{1,0:T(8,128)(2,1)} custom-call(bf16[1024,2048]{1,0:T(8,128)(2,1)} %tokens.1, f32[1,2048]{1,0:T(1,128)} %bitcast.4, bf16[2048,256]{1,0:T(8,128)(2,1)} %wq.1, bf16[2048,256]{1,0:T(8,128)(2,1)} %wf.1, bf16[2048,256]{1,0:T(8,128)(2,1)} %wi.1, bf16[2048,256]{1,0:T(8,128)(2,1)} %wg.1, bf16[2048,256]{1,0:T(8,128)(2,1)} %wh.1, ...), custom_call_target="tpu_custom_call" | custom-call | tf_op jit(solution)/shard_map/pallas_call | solution.py:301
  60.3 2.3 %copy.18 = bf16[1024,512]{1,0:T(8,128)(2,1)} copy(bf16[1024,512]{1,0:T(8,128)(2,1)} %shard_map.154) | data formatting | bytes 2097152
where the time goes:
time: 63.1 us; the launch traced here: 62.6 us
  Pallas kernels  60.3 us (96%)
  local copies, waits for them, and re-layouts  2.26 us (4%)
    pallas_call x1, Pallas kernels, body(): pl.pallas_call(functools.partial(fused_kernel, tp, sp), grid=(nb,), in_sp...  60.3 us
    unnamed x1, local copies, waits for them, and re-layouts  2.26 us

commit v1 on v0

v1 whole, which is shorter than its diff:
```python
import functools

import jax
import jax.numpy as jnp
from jax import lax
from jax.experimental import pallas as pl
from jax.experimental.pallas import tpu as pltpu
from jax.sharding import PartitionSpec as P

GROUP_FEATURES = 128
CHUNK = 128
ROWS = 256
TAPS = 3
HALO = 8
HEAD = 16
SHARE = 4
CONV, MIX = 0, 1

norm_eps = 1e-06
f32 = jnp.float32
bf16 = jnp.bfloat16


def dot(a, b, dims=((1,), (0,))):
    return lax.dot_general(a, b, (dims, ((), ())), preferred_element_type=f32)


def rms(values):
    return values * lax.rsqrt(jnp.mean(values * values, axis=-1, keepdims=True) + norm_eps)


def per_group(values, gain):
    parts = []
    for g in range(values.shape[1] // GROUP_FEATURES):
        parts.append(rms(values[:, g * GROUP_FEATURES : (g + 1) * GROUP_FEATURES]) * gain)
    return jnp.concatenate(parts, axis=1)


def head_slice(h):
    return slice(h * GROUP_FEATURES, (h + 1) * GROUP_FEATURES)


def prefix_sum(ones, values):
    high = values.astype(bf16)
    rest = values - high.astype(f32)
    middle = rest.astype(bf16)
    low = (rest - middle.astype(f32)).astype(bf16)
    return dot(ones, jnp.concatenate([high, middle, low], axis=0))


def fused_kernel(
    tp, sp, share,
    tokens, in_gain, wq, wf, wi, wg, wh, wb, wc, floor, leak, state_gain, taps, group_gain,
    out_state, out_conv, result,
    normed_all, w_scan, w_conv, w_read, cums, key_mid, value_all, olds, offsets,
    pad, state, offset, read, qdev, gate, conv_all, mix_all, columns, acc_all,
    sent_state, peer_state, peer_log, sent_total, sent_log, totals, total_logs,
    rim, tail, head_conv, head_gate, incoming,
    tok_sem, leak_sem, w_sem, own_sem,
    pair_send, pair_recv, piece_send, piece_recv, mate_send,
    blk_send, fwd_send, blk_recv, l1_send, l1_recv, l2_send, l2_recv, rim_send, rim_recv,
):
    me, place = lax.axis_index("tp"), lax.axis_index("sp")
    partner = me + 1 - 2 * lax.rem(me, 2)
    chips = tp // 2
    chip = lax.div(me, 2)
    core = lax.rem(me, 2)
    count, feats = normed_all.shape
    width = value_all.shape[1]
    channels = pad.shape[1]
    rows = ROWS
    nb = count // rows
    ncols = result.shape[1]
    heads = state.shape[0]
    piece = width // share
    mine = lax.rem(place, share)
    base = place - mine
    twin = place + 1 - 2 * lax.rem(place, 2)
    member = lax.rem(place, 2)
    pair = lax.div(place, 2)
    held = (conv_all, mix_all)
    outs = (out_conv, out_state)

    def block(t):
        return pl.ds(pl.multiple_of(t * rows, rows), rows)

    def token_copy(t):
        return pltpu.make_async_copy(tokens.at[block(t)], normed_all.at[block(t)], tok_sem.at[t])

    leak_copy = pltpu.make_async_copy(leak, cums, leak_sem.at[0])
    weights = ((wf, w_scan, 0), (wi, w_scan, 1), (wc, w_conv, 0), (wh, w_conv, 1),
               (wb, w_conv, 2), (wq, w_read, 0), (wg, w_read, 1))

    def weight_copy(n):
        src, dst, slot = weights[n]
        return pltpu.make_async_copy(
            src, dst.at[:, slot * width : (slot + 1) * width], w_sem.at[n]
        )

    def cols_of(device):
        return pl.ds(pl.multiple_of(device * ncols, ncols), ncols)

    def piece_rows(g):
        return pl.ds(pl.multiple_of(g * piece, piece), piece)

    def own_columns(kind):
        return pltpu.make_async_copy(
            outs[kind].at[:, cols_of(me)], columns.at[kind, me], own_sem.at[kind]
        )

    def pair_columns(kind, origin):
        return pltpu.make_async_remote_copy(
            outs[kind].at[:, cols_of(partner)], columns.at[kind, origin],
            pair_send.at[kind], pair_recv.at[kind], device_id={"tp": partner},
        )

    def far(k, c):
        return lax.rem(chip + k, chips) * 2 + c

    def piece_out(kind, k, c):
        target = far(k, c)
        return pltpu.make_async_remote_copy(
            outs[kind].at[piece_rows(mine), cols_of(target)],
            columns.at[kind, me, piece_rows(mine)],
            piece_send.at[kind, k, c], piece_recv.at[kind, me, mine], device_id={"tp": target},
        )

    def piece_in(kind, origin, g):
        ref = columns.at[kind, origin, piece_rows(g)]
        return pltpu.make_async_remote_copy(
            ref, ref, mate_send.at[kind, 0, 0, 0], piece_recv.at[kind, origin, g],
            device_id={"tp": partner},
        )

    def mate_copy(kind, k, c, r):
        ref = columns.at[kind, far(k, c), piece_rows(mine)]
        return pltpu.make_async_remote_copy(
            ref, ref, mate_send.at[kind, k, c, r], piece_recv.at[kind, far(k, c), mine],
            device_id={"sp": base + lax.rem(mine + r, share)},
        )

    far_devices = [(k, c) for k in range(1, chips) for c in range(2)]

    def span(kind, t):
        if kind == CONV and isinstance(t, int):
            if t == 0:
                return pl.ds(HEAD, rows - HEAD)
            if t == nb:
                return pl.ds(0, HEAD)
        return block(t)

    def block_copy(kind, t, origin, target, send):
        ref = held[kind].at[origin, span(kind, t)]
        return pltpu.make_async_remote_copy(
            ref, ref, send, blk_recv.at[kind, origin, t], device_id={"tp": target}
        )

    def own_copies(kind, t):
        out = []
        for k in range(1, chips):
            out.append(block_copy(kind, t, me, far(k, core), blk_send.at[kind, k, t]))
        out.append(block_copy(kind, t, me, partner, blk_send.at[kind, 0, t]))
        return out

    def relays(kind, t):
        return [
            block_copy(kind, t, far(k, core), partner, fwd_send.at[kind, k, t])
            for k in range(1, chips)
        ]

    def start(copies):
        for copy in copies:
            copy.start()

    def relay(kind, t):
        for copy in relays(kind, t):
            copy.wait_recv()
            copy.start()

    def arrived(kind, t, origin):
        block_copy(kind, t, origin, partner, blk_send.at[kind, 0, t]).wait_recv()

    def twin_copies():
        to = {"sp": twin}
        return (
            pltpu.make_async_remote_copy(
                sent_state, peer_state, l1_send.at[0], l1_recv.at[0], device_id=to
            ),
            pltpu.make_async_remote_copy(
                offset, peer_log, l1_send.at[1], l1_recv.at[1], device_id=to
            ),
        )

    def total_copies(k, source):
        to = {"sp": lax.rem(place + 2 * k, sp)}
        return (
            pltpu.make_async_remote_copy(
                sent_total, totals.at[source], l2_send.at[0, k], l2_recv.at[0, source],
                device_id=to,
            ),
            pltpu.make_async_remote_copy(
                sent_log, total_logs.at[source], l2_send.at[1, k], l2_recv.at[1, source],
                device_id=to,
            ),
        )

    rim_copy = pltpu.make_async_remote_copy(
        tail, rim, rim_send.at[0], rim_recv.at[0], device_id={"sp": lax.rem(place + 1, sp)}
    )

    token_copy(0).start()
    weight_copy(0).start()
    weight_copy(1).start()
    leak_copy.start()
    for t in range(1, nb):
        token_copy(t).start()
    for n in range(2, 7):
        weight_copy(n).start()
    barrier = pltpu.get_barrier_semaphore()
    for k in range(1, tp):
        pl.semaphore_signal(barrier, inc=1, device_id={"tp": lax.rem(me + k, tp)})
    for k in range(1, sp):
        pl.semaphore_signal(barrier, inc=1, device_id={"sp": lax.rem(place + k, sp)})
    pl.semaphore_wait(barrier, tp + sp - 2)
    for kind in (CONV, MIX):
        for k, c in far_devices:
            piece_out(kind, k, c).start()
    for kind in (CONV, MIX):
        pair_columns(kind, me).start()
        own_columns(kind).start()

    state[...] = jnp.zeros_like(state)
    offset[...] = jnp.zeros_like(offset)
    pad[0:HALO, :] = jnp.zeros((HALO, channels), f32)

    r = lax.broadcasted_iota(jnp.int32, (CHUNK, CHUNK), 0)
    c = lax.broadcasted_iota(jnp.int32, (CHUNK, CHUNK), 1)
    causal = r >= c
    ones = jnp.concatenate([causal.astype(f32)] * 3, axis=1).astype(bf16)
    w_taps = taps[...].astype(f32)

    weight_copy(0).wait()
    weight_copy(1).wait()
    leak_copy.wait()

    def scan_block(t, _):
        token_copy(t).wait()
        at = block(t)
        normed = (rms(normed_all[at, :].astype(f32)) * in_gain[...]).astype(bf16)
        normed_all[at, :] = normed
        both = dot(normed, w_scan[...])
        x = both[:, :width].astype(bf16).astype(f32)
        value = both[:, width:].astype(bf16)
        value_all[at, :] = value
        key = (1.0 - floor[...]) * jax.nn.sigmoid(-x)
        logf = jnp.log(1.0 - key) + cums[at, :]
        for b in range(rows // CHUNK):
            lo, hi = b * CHUNK, (b + 1) * CHUNK
            where = pl.ds(pl.multiple_of(t * rows + lo, CHUNK), CHUNK)
            number = t * (rows // CHUNK) + b
            cum = prefix_sum(ones, logf[lo:hi])
            mid = cum[CHUNK // 2 - 1 : CHUNK // 2]
            last = cum[CHUNK - 1 : CHUNK]
            k_mid = key[lo:hi] * jnp.exp(mid - cum)
            k_end = (k_mid * jnp.exp(last - mid)).astype(bf16)
            cums[where, :] = cum
            key_mid[where, :] = k_mid.astype(bf16)
            offsets[number] = offset[...]
            for h in range(heads):
                s = head_slice(h)
                old = state[h]
                olds[number, h] = old.astype(bf16)
                state[h] = old * jnp.exp(last[:, s]) + dot(
                    value[lo:hi, s], k_end[:, s], ((0,), (0,))
                )
            offset[...] += last
        return 0

    lax.fori_loop(0, nb, scan_block, 0)
    sent_state[...] = state[...].astype(bf16)
    start(twin_copies())

    for n in (2, 3, 4):
        weight_copy(n).wait()

    def conv_block(t, _):
        at = block(t)
        three = dot(normed_all[at, :], w_conv[...])
        first = three[:, :channels].astype(bf16).astype(f32)
        second = three[:, channels : 2 * channels].astype(bf16).astype(f32)
        proj_b = three[:, 2 * channels :].astype(bf16).astype(f32)
        conv_in = (first * second).astype(bf16).astype(f32)
        pad[HALO : HALO + rows, :] = conv_in
        total = w_taps[TAPS - 1 : TAPS] * conv_in
        for j in range(TAPS - 1):
            lo = HALO - (TAPS - 1) + j
            total += w_taps[j : j + 1] * pad[lo : lo + rows, :]
        conv_all[me, at, :] = per_group(proj_b * total, group_gain[...]).astype(bf16)

        @pl.when(t == 0)
        def _():
            head_conv[...] = conv_in[:HALO]
            head_gate[...] = proj_b[:HALO]
            start(own_copies(CONV, 0))

        @pl.when(t > 0)
        def _():
            start(own_copies(CONV, t))

        pad[0:HALO, :] = conv_in[rows - HALO :]

        @pl.when(t == nb - 1)
        def _():
            tail[...] = conv_in[rows - HALO :]
            rim_copy.start()

        @pl.when(t == min(2, nb - 1))
        def _():
            for copy in twin_copies():
                copy.wait_recv()
            log_second = jnp.where(member == 0, peer_log[0:1, :], offset[0:1, :])
            decay = jnp.exp(log_second)
            for h in range(heads):
                own, other = state[h], peer_state[h].astype(f32)
                early = jnp.where(member == 0, own, other)
                late = jnp.where(member == 0, other, own)
                sent_total[h] = (early * decay[:, head_slice(h)] + late).astype(bf16)
            sent_log[...] = offset[...] + peer_log[...]
            for k in range(1, sp // 2):
                @pl.when(pair + k < sp // 2)
                def _():
                    start(total_copies(k, pair))

        return 0

    lax.fori_loop(0, nb, conv_block, 0)

    for n in (5, 6):
        weight_copy(n).wait()

    def read_block(t, _):
        at = block(t)
        both = dot(normed_all[at, :], w_read[...])
        query = jax.nn.silu(both[:, :width].astype(bf16).astype(f32))
        outgate = jax.nn.silu(both[:, width:].astype(bf16).astype(f32))
        for h in range(heads):
            s = head_slice(h)
            gate[at, s] = outgate[:, s] * state_gain[...]
        for b in range(rows // CHUNK):
            lo, hi = b * CHUNK, (b + 1) * CHUNK
            where = pl.ds(pl.multiple_of(t * rows + lo, CHUNK), CHUNK)
            number = t * (rows // CHUNK) + b
            cum = cums[where, :]
            mid = cum[CHUNK // 2 - 1 : CHUNK // 2]
            q_mid = query[lo:hi] * jnp.exp(cum - mid)
            q_all = q_mid * jnp.exp(mid)
            qdev[where, :] = (q_all * jnp.exp(offsets[number, 0:1, :])).astype(bf16)
            q_mid, q_all = q_mid.astype(bf16), q_all.astype(bf16)
            for h in range(heads):
                s = head_slice(h)
                scores = dot(q_mid[:, s], key_mid[where, s], ((1,), (1,)))
                scores = jnp.where(causal, scores, 0.0).astype(bf16)
                read[where, s] = dot(scores, value_all[where, s]) + dot(
                    q_all[:, s], olds[number, h], ((1,), (1,))
                )

        @pl.when(t == 0)
        def _():
            rim_copy.wait_recv()
            before = jnp.where(place > 0, rim[...], 0.0)
            ext = jnp.concatenate([before, head_conv[...]], axis=0)
            fixed = w_taps[TAPS - 1 : TAPS] * head_conv[...]
            for j in range(TAPS - 1):
                lo = HALO - (TAPS - 1) + j
                fixed += w_taps[j : j + 1] * ext[lo : lo + HALO]
            fixed = per_group(head_gate[...] * fixed, group_gain[...])
            conv_all[me, 0:HALO, :] = fixed.astype(bf16)
            start(own_copies(CONV, nb))

        return 0

    lax.fori_loop(0, nb, read_block, 0)

    for kind in (CONV, MIX):
        for k, c in far_devices:
            piece_in(kind, far(k, c), mine).wait_recv()
            for n in range(1, share):
                mate_copy(kind, k, c, n).start()
    for kind in (CONV, MIX):
        own_columns(kind).wait()
        pair_columns(kind, partner).wait_recv()

    def near(kind, t):
        out = dot(held[kind][me, block(t), :], columns[kind, me])
        return out + dot(held[kind][partner, block(t), :], columns[kind, partner])

    def near_conv(t, _):
        acc_all[block(t), :] = near(CONV, t)
        return 0

    arrived(CONV, 0, partner)
    arrived(CONV, nb, partner)

    def conv_partner(t, _):
        arrived(CONV, t + 1, partner)
        return 0

    lax.fori_loop(0, nb - 1, conv_partner, 0)
    lax.fori_loop(0, nb, near_conv, 0)

    for k in range(1, sp // 2):
        @pl.when(pair >= k)
        def _():
            for copy in total_copies(k, pair - k):
                copy.wait_recv()
    incoming[...] = jnp.zeros_like(incoming)

    def hop(p, _):
        decay = jnp.exp(total_logs[p, 0:1, :])
        for h in range(heads):
            incoming[h] = incoming[h] * decay[:, head_slice(h)] + totals[p, h].astype(f32)
        return 0

    lax.fori_loop(0, pair, hop, 0)
    decay = jnp.exp(peer_log[0:1, :])
    for h in range(heads):
        through = incoming[h] * decay[:, head_slice(h)] + peer_state[h].astype(f32)
        incoming[h] = jnp.where(member == 0, incoming[h], through)

    def merge(t, _):
        at = block(t)
        for h in range(heads):
            s = head_slice(h)
            whole = read[at, s] + dot(qdev[at, s], incoming[h].astype(bf16), ((1,), (1,)))
            mix_all[me, at, s] = (rms(whole) * gate[at, s]).astype(bf16)
        start(own_copies(MIX, t))
        return 0

    lax.fori_loop(0, nb, merge, 0)

    def near_mix(t, _):
        arrived(MIX, t, partner)
        acc_all[block(t), :] += near(MIX, t)
        return 0

    lax.fori_loop(0, nb, near_mix, 0)

    def conv_relay(t, _):
        relay(CONV, t + 1)
        return 0

    relay(CONV, 0)
    lax.fori_loop(0, nb - 1, conv_relay, 0)
    relay(CONV, nb)
    for kind in (CONV, MIX):
        for k, c in far_devices:
            for n in range(1, share):
                piece_in(kind, far(k, c), lax.rem(mine + n, share)).wait_recv()
    for k in range(1, chips):
        arrived(CONV, 0, far(k, 1 - core))
        arrived(CONV, nb, far(k, 1 - core))

    def conv_arrivals(t, _):
        for k in range(1, chips):
            arrived(CONV, t + 1, far(k, 1 - core))
        return 0

    lax.fori_loop(0, nb - 1, conv_arrivals, 0)

    def far_conv(t, _):
        acc = acc_all[block(t), :]
        for k, c in far_devices:
            origin = far(k, c)
            acc += dot(conv_all[origin, block(t), :], columns[CONV, origin])
        acc_all[block(t), :] = acc
        return 0

    lax.fori_loop(0, nb, far_conv, 0)

    def finish(t, _):
        relay(MIX, t)
        for k in range(1, chips):
            arrived(MIX, t, far(k, 1 - core))
        acc = acc_all[block(t), :]
        for k, c in far_devices:
            origin = far(k, c)
            acc += dot(mix_all[origin, block(t), :], columns[MIX, origin])
        result[block(t), :] = acc.astype(bf16)
        return 0

    lax.fori_loop(0, nb, finish, 0)

    def drain(t, _):
        for copy in own_copies(MIX, t) + relays(MIX, t):
            copy.wait_send()
        return 0

    def drain_conv(t, _):
        for copy in own_copies(CONV, t + 1) + relays(CONV, t + 1):
            copy.wait_send()
        return 0

    lax.fori_loop(0, nb, drain, 0)
    lax.fori_loop(0, nb - 1, drain_conv, 0)
    for t in (0, nb):
        for copy in own_copies(CONV, t) + relays(CONV, t):
            copy.wait_send()
    for kind in (CONV, MIX):
        pair_columns(kind, me).wait_send()
        for k, c in far_devices:
            piece_out(kind, k, c).wait_send()
            for n in range(1, share):
                mate_copy(kind, k, c, n).wait_send()
    rim_copy.wait_send()
    for copy in twin_copies():
        copy.wait_send()
    for k in range(1, sp // 2):
        @pl.when(pair + k < sp // 2)
        def _():
            for copy in total_copies(k, pair):
                copy.wait_send()


def body(
    tokens, in_gain, w_query, w_forget, w_input, w_outgate, w_conv_h, w_conv_b, w_conv_c,
    forget_floor, forget_leak, state_gain, conv_taps, group_gain, out_state, out_conv,
):
    count, feats = tokens.shape
    width, channels = w_query.shape[1], w_conv_h.shape[1]
    heads = width // GROUP_FEATURES
    tp, sp = lax.axis_size("tp"), lax.axis_size("sp")
    ncols, nb, chips = out_state.shape[1] // tp, count // ROWS, tp // 2
    share = min(SHARE, sp)
    chunks, pairs = count // CHUNK, sp // 2

    hbm = pl.BlockSpec(memory_space=pl.ANY)
    vmem = pl.BlockSpec(memory_space=pltpu.VMEM)
    sems = pltpu.SemaphoreType.DMA
    square = (heads, GROUP_FEATURES, GROUP_FEATURES)
    return pl.pallas_call(
        functools.partial(fused_kernel, tp, sp, share),
        in_specs=[hbm, vmem] + [hbm] * 7 + [vmem, hbm, vmem, vmem, vmem, hbm, hbm],
        out_specs=vmem,
        out_shape=jax.ShapeDtypeStruct((count, ncols), bf16),
        scratch_shapes=[
            pltpu.VMEM((count, feats), bf16),
            pltpu.VMEM((feats, 2 * width), bf16),
            pltpu.VMEM((feats, 3 * channels), bf16),
            pltpu.VMEM((feats, 2 * width), bf16),
            pltpu.VMEM((count, width), f32),
            pltpu.VMEM((count, width), bf16),
            pltpu.VMEM((count, width), bf16),
            pltpu.VMEM((chunks,) + square, bf16),
            pltpu.VMEM((chunks, HALO, width), f32),
            pltpu.VMEM((HALO + ROWS, channels), f32),
            pltpu.VMEM(square, f32),
            pltpu.VMEM((HALO, width), f32),
            pltpu.VMEM((count, width), f32),
            pltpu.VMEM((count, width), bf16),
            pltpu.VMEM((count, width), f32),
            pltpu.VMEM((tp, count, channels), bf16),
            pltpu.VMEM((tp, count, width), bf16),
            pltpu.VMEM((2, tp, width, ncols), bf16),
            pltpu.VMEM((count, ncols), f32),
            pltpu.VMEM(square, bf16),
            pltpu.VMEM(square, bf16),
            pltpu.VMEM((HALO, width), f32),
            pltpu.VMEM(square, bf16),
            pltpu.VMEM((HALO, width), f32),
            pltpu.VMEM((pairs,) + square, bf16),
            pltpu.VMEM((pairs, HALO, width), f32),
            pltpu.VMEM((HALO, channels), f32),
            pltpu.VMEM((HALO, channels), f32),
            pltpu.VMEM((HALO, channels), f32),
            pltpu.VMEM((HALO, channels), f32),
            pltpu.VMEM(square, f32),
            sems((nb,)), sems((1,)), sems((7,)), sems((2,)),
            sems((2,)), sems((2,)), sems((2, chips, 2)), sems((2, tp, share)),
            sems((2, chips, 2, share)),
            sems((2, chips, nb + 1)), sems((2, chips, nb + 1)), sems((2, tp, nb + 1)),
            sems((2,)), sems((2,)), sems((2, pairs)), sems((2, pairs)), sems((1,)), sems((1,)),
        ],
        compiler_params=pltpu.CompilerParams(
            vmem_limit_bytes=56 * 2**20, collective_id=0, has_side_effects=True
        ),
    )(
        tokens, in_gain[None], w_query, w_forget, w_input, w_outgate, w_conv_h, w_conv_b, w_conv_c,
        forget_floor[None], forget_leak, state_gain[None], conv_taps, group_gain[None],
        out_state, out_conv,
    )


def solution(mesh):
    cols, rows = P(None, "tp"), P("tp", None)
    in_specs = (
        P("sp", None), P(), cols, cols, cols, cols, cols, cols, cols,
        P("tp"), P("sp", "tp"), P(), cols, P(), rows, rows,
    )
    return jax.shard_map(
        body, mesh=mesh, in_specs=in_specs, out_specs=P("sp", "tp"), check_vma=False
    )
```

time: 63.1 us -> 51 us (0.81)
  Pallas kernels: 60.3 us -> 47.9 us
    pallas_call x1, Pallas kernels: 60.3 us -> 47.9 us  [body(): pl.pallas_call(functools.partial(fused_kernel, tp, sp, share), in_specs=[...]
where the time goes in v1:
time: 51 us; the launch traced here: 50.1 us
  Pallas kernels  47.9 us (94%)
  local copies, waits for them, and re-layouts  2.26 us (4%)
    pallas_call x1, Pallas kernels, body(): pl.pallas_call(functools.partial(fused_kernel, tp, sp, share), in_specs=[...  47.9 us
    unnamed x1, local copies, waits for them, and re-layouts  2.26 us

profile of v1, /device:TPU:1, one launch (start us, length us, event | category | flops | bytes accessed | tf_op | source)
XLA Modules:
  0.0 50.1 jit_solution(17379786820007266893)
XLA Ops:
  0.0 47.9 %shard_map.154 = bf16[1024,512]{1,0:T(8,128)(2,1)} custom-call(bf16[1024,2048]{1,0:T(8,128)(2,1)} %tokens.1, f32[1,2048]{1,0:T(1,128)} %bitcast.4, bf16[2048,256]{1,0:T(8,128)(2,1)} %wq.1, bf16[2048,256]{1,0:T(8,128)(2,1)} %wf.1, bf16[2048,256]{1,0:T(8,128)(2,1)} %wi.1, bf16[2048,256]{1,0:T(8,128)(2,1)} %wg.1, bf16[2048,256]{1,0:T(8,128)(2,1)} %wh.1, ...), custom_call_target="tpu_custom_call" | custom-call | tf_op jit(solution)/shard_map/pallas_call | solution.py:540
  47.9 2.3 %copy.18 = bf16[1024,512]{1,0:T(8,128)(2,1)} copy(bf16[1024,512]{1,0:T(8,128)(2,1)} %shard_map.154) | data formatting | bytes 2097152

commit v2 on v1

--- a/solution.py
+++ b/solution.py
@@ -58,7 +58,7 @@
     rim, tail, head_conv, head_gate, incoming,
     tok_sem, leak_sem, w_sem, own_sem,
     pair_send, pair_recv, piece_send, piece_recv, mate_send,
-    blk_send, fwd_send, blk_recv, l1_send, l1_recv, l2_send, l2_recv, rim_send, rim_recv,
+    blk_send, fwd_send, blk_recv, l1_send, l1_recv, l2_send, l2_recv, rim_send, rim_recv, ready, rim_ready,
 ):
     me, place = lax.axis_index("tp"), lax.axis_index("sp")
     partner = me + 1 - 2 * lax.rem(me, 2)
@@ -74,10 +74,14 @@
     heads = state.shape[0]
     piece = width // share
     mine = lax.rem(place, share)
-    base = place - mine
     twin = place + 1 - 2 * lax.rem(place, 2)
+    across = share // 2
+    step = across - share * lax.div(mine, across)
+    mate, mates_piece = place + step, mine + step
     member = lax.rem(place, 2)
     pair = lax.div(place, 2)
+    pairs = sp // 2
+    before, after = lax.rem(place + sp - 1, sp), lax.rem(place + 1, sp)
     held = (conv_all, mix_all)
     outs = (out_conv, out_state)
 
@@ -87,7 +91,9 @@
     def token_copy(t):
         return pltpu.make_async_copy(tokens.at[block(t)], normed_all.at[block(t)], tok_sem.at[t])
 
-    leak_copy = pltpu.make_async_copy(leak, cums, leak_sem.at[0])
+    def leak_copy(t):
+        return pltpu.make_async_copy(leak.at[block(t)], cums.at[block(t)], leak_sem.at[t])
+
     weights = ((wf, w_scan, 0), (wi, w_scan, 1), (wc, w_conv, 0), (wh, w_conv, 1),
                (wb, w_conv, 2), (wq, w_read, 0), (wg, w_read, 1))
 
@@ -132,12 +138,24 @@
             device_id={"tp": partner},
         )
 
-    def mate_copy(kind, k, c, r):
-        ref = columns.at[kind, far(k, c), piece_rows(mine)]
+    def pass_on(kind, k, c, n):
+        g, to = ((mine, mate), (mine, twin), (mates_piece, twin))[n]
+        ref = columns.at[kind, far(k, c), piece_rows(g)]
         return pltpu.make_async_remote_copy(
-            ref, ref, mate_send.at[kind, k, c, r], piece_recv.at[kind, far(k, c), mine],
-            device_id={"sp": base + lax.rem(mine + r, share)},
-        )
+            ref, ref, mate_send.at[kind, k, c, n], piece_recv.at[kind, far(k, c), g],
+            device_id={"sp": to},
+        )
+
+    def pass_own(kind):
+        for k, c in far_devices:
+            piece_in(kind, far(k, c), mine).wait_recv()
+            pass_on(kind, k, c, 0).start()
+            pass_on(kind, k, c, 1).start()
+
+    def pass_mates(kind):
+        for k, c in far_devices:
+            piece_in(kind, far(k, c), mates_piece).wait_recv()
+            pass_on(kind, k, c, 2).start()
 
     far_devices = [(k, c) for k in range(1, chips) for c in range(2)]
 
@@ -187,7 +205,7 @@
                 sent_state, peer_state, l1_send.at[0], l1_recv.at[0], device_id=to
             ),
             pltpu.make_async_remote_copy(
-                offset, peer_log, l1_send.at[1], l1_recv.at[1], device_id=to
+                offset.at[0:1], peer_log.at[0:1], l1_send.at[1], l1_recv.at[1], device_id=to
             ),
         )
 
@@ -199,29 +217,44 @@
                 device_id=to,
             ),
             pltpu.make_async_remote_copy(
-                sent_log, total_logs.at[source], l2_send.at[1, k], l2_recv.at[1, source],
+                sent_log.at[0:1], total_logs.at[source, 0:1], l2_send.at[1, k], l2_recv.at[1, source],
                 device_id=to,
             ),
         )
 
     rim_copy = pltpu.make_async_remote_copy(
-        tail, rim, rim_send.at[0], rim_recv.at[0], device_id={"sp": lax.rem(place + 1, sp)}
+        tail, rim, rim_send.at[0], rim_recv.at[0], device_id={"sp": after}
     )
 
     token_copy(0).start()
     weight_copy(0).start()
     weight_copy(1).start()
-    leak_copy.start()
-    for t in range(1, nb):
-        token_copy(t).start()
-    for n in range(2, 7):
-        weight_copy(n).start()
+    leak_copy(0).start()
     barrier = pltpu.get_barrier_semaphore()
     for k in range(1, tp):
         pl.semaphore_signal(barrier, inc=1, device_id={"tp": lax.rem(me + k, tp)})
-    for k in range(1, sp):
-        pl.semaphore_signal(barrier, inc=1, device_id={"sp": lax.rem(place + k, sp)})
-    pl.semaphore_wait(barrier, tp + sp - 2)
+    for to in (twin, mate):
+        pl.semaphore_signal(barrier, inc=1, device_id={"sp": to})
+    for k in range(1, pairs):
+        @pl.when(pair + k < pairs)
+        def _():
+            pl.semaphore_signal(barrier, inc=1, device_id={"sp": lax.rem(place + 2 * k, sp)})
+    follows = jnp.logical_and(member == 0, pair > 0)
+    leads = jnp.logical_and(member == 1, pair < pairs - 1)
+
+    @pl.when(leads)
+    def _():
+        pl.semaphore_signal(barrier, inc=1, device_id={"sp": after})
+
+    pl.semaphore_wait(barrier, tp + 1 + pair + jnp.where(follows, 1, 0))
+    for k in range(1, pairs):
+        @pl.when(pair >= k)
+        def _():
+            pl.semaphore_signal(ready, inc=1, device_id={"sp": lax.rem(place + sp - 2 * k, sp)})
+
+    @pl.when(follows)
+    def _():
+        pl.semaphore_signal(rim_ready, inc=1, device_id={"sp": before})
     for kind in (CONV, MIX):
         for k, c in far_devices:
             piece_out(kind, k, c).start()
@@ -241,10 +274,15 @@
 
     weight_copy(0).wait()
     weight_copy(1).wait()
-    leak_copy.wait()
+    for t in range(1, nb):
+        token_copy(t).start()
+        leak_copy(t).start()
+    for n in range(2, 7):
+        weight_copy(n).start()
 
     def scan_block(t, _):
         token_copy(t).wait()
+        leak_copy(t).wait()
         at = block(t)
         normed = (rms(normed_all[at, :].astype(f32)) * in_gain[...]).astype(bf16)
         normed_all[at, :] = normed
@@ -279,6 +317,8 @@
     lax.fori_loop(0, nb, scan_block, 0)
     sent_state[...] = state[...].astype(bf16)
     start(twin_copies())
+    pass_own(CONV)
+    pass_own(MIX)
 
     for n in (2, 3, 4):
         weight_copy(n).wait()
@@ -312,7 +352,16 @@
         @pl.when(t == nb - 1)
         def _():
             tail[...] = conv_in[rows - HALO :]
-            rim_copy.start()
+
+            @pl.when(leads)
+            def _():
+                pl.semaphore_wait(rim_ready, 1)
+
+            @pl.when(place < sp - 1)
+            def _():
+                rim_copy.start()
+
+            pass_mates(CONV)
 
         @pl.when(t == min(2, nb - 1))
         def _():
@@ -325,9 +374,14 @@
                 early = jnp.where(member == 0, own, other)
                 late = jnp.where(member == 0, other, own)
                 sent_total[h] = (early * decay[:, head_slice(h)] + late).astype(bf16)
-            sent_log[...] = offset[...] + peer_log[...]
-            for k in range(1, sp // 2):
-                @pl.when(pair + k < sp // 2)
+            sent_log[0:1, :] = offset[0:1, :] + peer_log[0:1, :]
+
+            @pl.when(pair < pairs - 1)
+            def _():
+                pl.semaphore_wait(ready, pairs - 1 - pair)
+
+            for k in range(1, pairs):
+                @pl.when(pair + k < pairs)
                 def _():
                     start(total_copies(k, pair))
 
@@ -364,11 +418,17 @@
                     q_all[:, s], olds[number, h], ((1,), (1,))
                 )
 
-        @pl.when(t == 0)
-        def _():
-            rim_copy.wait_recv()
-            before = jnp.where(place > 0, rim[...], 0.0)
-            ext = jnp.concatenate([before, head_conv[...]], axis=0)
+        @pl.when(t == nb - 1)
+        def _():
+            @pl.when(place == 0)
+            def _():
+                rim[...] = jnp.zeros_like(rim)
+
+            @pl.when(place > 0)
+            def _():
+                rim_copy.wait_recv()
+
+            ext = jnp.concatenate([rim[...], head_conv[...]], axis=0)
             fixed = w_taps[TAPS - 1 : TAPS] * head_conv[...]
             for j in range(TAPS - 1):
                 lo = HALO - (TAPS - 1) + j
@@ -376,39 +436,13 @@
             fixed = per_group(head_gate[...] * fixed, group_gain[...])
             conv_all[me, 0:HALO, :] = fixed.astype(bf16)
             start(own_copies(CONV, nb))
+            pass_mates(MIX)
 
         return 0
 
     lax.fori_loop(0, nb, read_block, 0)
 
-    for kind in (CONV, MIX):
-        for k, c in far_devices:
-            piece_in(kind, far(k, c), mine).wait_recv()
-            for n in range(1, share):
-                mate_copy(kind, k, c, n).start()
-    for kind in (CONV, MIX):
-        own_columns(kind).wait()
-        pair_columns(kind, partner).wait_recv()
-
-    def near(kind, t):
-        out = dot(held[kind][me, block(t), :], columns[kind, me])
-        return out + dot(held[kind][partner, block(t), :], columns[kind, partner])
-
-    def near_conv(t, _):
-        acc_all[block(t), :] = near(CONV, t)
-        return 0
-
-    arrived(CONV, 0, partner)
-    arrived(CONV, nb, partner)
-
-    def conv_partner(t, _):
-        arrived(CONV, t + 1, partner)
-        return 0
-
-    lax.fori_loop(0, nb - 1, conv_partner, 0)
-    lax.fori_loop(0, nb, near_conv, 0)
-
-    for k in range(1, sp // 2):
+    for k in range(1, pairs):
         @pl.when(pair >= k)
         def _():
             for copy in total_copies(k, pair - k):
@@ -438,6 +472,29 @@
 
     lax.fori_loop(0, nb, merge, 0)
 
+    for kind in (CONV, MIX):
+        own_columns(kind).wait()
+        pair_columns(kind, partner).wait_recv()
+
+    def near(kind, t):
+        out = dot(held[kind][me, block(t), :], columns[kind, me])
+        return out + dot(held[kind][partner, block(t), :], columns[kind, partner])
+
+    def near_conv(t, _):
+        acc_all[block(t), :] = near(CONV, t)
+        return 0
+
+    arrived(CONV, 0, partner)
+    arrived(CONV, nb, partner)
+
+    def conv_partner(t, _):
+        arrived(CONV, t + 1, partner)
+        return 0
+
+    lax.fori_loop(0, nb - 1, conv_partner, 0)
+    lax.fori_loop(0, nb, near_conv, 0)
+
+
     def near_mix(t, _):
         arrived(MIX, t, partner)
         acc_all[block(t), :] += near(MIX, t)
@@ -454,8 +511,8 @@
     relay(CONV, nb)
     for kind in (CONV, MIX):
         for k, c in far_devices:
-            for n in range(1, share):
-                piece_in(kind, far(k, c), lax.rem(mine + n, share)).wait_recv()
+            for g in (mine + 1 - 2 * lax.rem(mine, 2), mates_piece + 1 - 2 * lax.rem(mine, 2)):
+                piece_in(kind, far(k, c), g).wait_recv()
     for k in range(1, chips):
         arrived(CONV, 0, far(k, 1 - core))
         arrived(CONV, nb, far(k, 1 - core))
@@ -509,13 +566,17 @@
         pair_columns(kind, me).wait_send()
         for k, c in far_devices:
             piece_out(kind, k, c).wait_send()
-            for n in range(1, share):
-                mate_copy(kind, k, c, n).wait_send()
-    rim_copy.wait_send()
+            for n in range(3):
+                pass_on(kind, k, c, n).wait_send()
+
+    @pl.when(place < sp - 1)
+    def _():
+        rim_copy.wait_send()
+
     for copy in twin_copies():
         copy.wait_send()
-    for k in range(1, sp // 2):
-        @pl.when(pair + k < sp // 2)
+    for k in range(1, pairs):
+        @pl.when(pair + k < pairs)
         def _():
             for copy in total_copies(k, pair):
                 copy.wait_send()
@@ -533,7 +594,7 @@
     share = min(SHARE, sp)
     chunks, pairs = count // CHUNK, sp // 2
 
-    hbm = pl.BlockSpec(memory_space=pl.ANY)
+    hbm = pl.BlockSpec(memory_space=pltpu.HBM)
     vmem = pl.BlockSpec(memory_space=pltpu.VMEM)
     sems = pltpu.SemaphoreType.DMA
     square = (heads, GROUP_FEATURES, GROUP_FEATURES)
@@ -541,7 +602,7 @@
         functools.partial(fused_kernel, tp, sp, share),
         in_specs=[hbm, vmem] + [hbm] * 7 + [vmem, hbm, vmem, vmem, vmem, hbm, hbm],
         out_specs=vmem,
-        out_shape=jax.ShapeDtypeStruct((count, ncols), bf16),
+        out_shape=pltpu.VMEM((count, ncols), bf16),
         scratch_shapes=[
             pltpu.VMEM((count, feats), bf16),
             pltpu.VMEM((feats, 2 * width), bf16),
@@ -574,11 +635,12 @@
             pltpu.VMEM((HALO, channels), f32),
             pltpu.VMEM((HALO, channels), f32),
             pltpu.VMEM(square, f32),
-            sems((nb,)), sems((1,)), sems((7,)), sems((2,)),
+            sems((nb,)), sems((nb,)), sems((7,)), sems((2,)),
             sems((2,)), sems((2,)), sems((2, chips, 2)), sems((2, tp, share)),
-            sems((2, chips, 2, share)),
+            sems((2, chips, 2, 3)),
             sems((2, chips, nb + 1)), sems((2, chips, nb + 1)), sems((2, tp, nb + 1)),
             sems((2,)), sems((2,)), sems((2, pairs)), sems((2, pairs)), sems((1,)), sems((1,)),
+            pltpu.SemaphoreType.REGULAR, pltpu.SemaphoreType.REGULAR,
         ],
         compiler_params=pltpu.CompilerParams(
             vmem_limit_bytes=56 * 2**20, collective_id=0, has_side_effects=True

time: 51 us -> 40.9 us (0.80); the launches traced: 50.1 us -> 40.8 us
  Pallas kernels: 47.9 us -> 39.8 us
  local copies, waits for them, and re-layouts: 2.26 us -> 0.97 us
    pallas_call x1, Pallas kernels: 47.9 us -> 39.8 us  [body(): pl.pallas_call(functools.partial(fused_kernel, tp, sp, share), in_specs=[...]
    unnamed x1, local copies, waits for them, and re-layouts: 2.26 us -> 0.97 us
where the time goes in v2:
time: 40.9 us; the launch traced here: 40.8 us
  Pallas kernels  39.8 us (97%)
  local copies, waits for them, and re-layouts  0.97 us (2%)
    pallas_call x1, Pallas kernels, body(): pl.pallas_call(functools.partial(fused_kernel, tp, sp, share), in_specs=[...  39.8 us
    unnamed x1, local copies, waits for them, and re-layouts  0.97 us

profile of v2, /device:TPU:1, one launch (start us, length us, event | category | flops | bytes accessed | tf_op | source)
XLA Modules:
  0.0 40.8 jit_solution(8578846987923138009)
XLA Ops:
  0.0 39.8 %shard_map.154 = bf16[1024,512]{1,0:T(8,128)(2,1)S(1)} custom-call(bf16[1024,2048]{1,0:T(8,128)(2,1)} %tokens.1, f32[1,2048]{1,0:T(1,128)} %bitcast.4, bf16[2048,256]{1,0:T(8,128)(2,1)} %wq.1, bf16[2048,256]{1,0:T(8,128)(2,1)} %wf.1, bf16[2048,256]{1,0:T(8,128)(2,1)} %wi.1, bf16[2048,256]{1,0:T(8,128)(2,1)} %wg.1, bf16[2048,256]{1,0:T(8,128)(2,1)} %wh.1, ...), custom_call_target="tpu_custom_call" | custom-call | tf_op jit(solution)/shard_map/pallas_call | solution.py:601
  39.8 1.0 %copy.18 = bf16[1024,512]{1,0:T(8,128)(2,1)} copy(bf16[1024,512]{1,0:T(8,128)(2,1)S(1)} %shard_map.154) | data formatting | bytes 2097152

commit v3 on v2

v3 whole, which is shorter than its diff:
```python
import functools

import jax
import jax.numpy as jnp
from jax import lax
from jax.experimental import pallas as pl
from jax.experimental.pallas import tpu as pltpu
from jax.sharding import PartitionSpec as P

GROUP_FEATURES = 128
CHUNK = 128
ROWS = 256
MIX_ROWS = 128
LAG = 2
EXTRA = 16
TAPS = 3
HALO = 8
HEAD = 16
SHARE = 4
CONV, MIX = 0, 1

norm_eps = 1e-06
f32 = jnp.float32
bf16 = jnp.bfloat16


def dot(a, b, dims=((1,), (0,))):
    return lax.dot_general(a, b, (dims, ((), ())), preferred_element_type=f32)


def rms(values):
    return values * lax.rsqrt(jnp.mean(values * values, axis=-1, keepdims=True) + norm_eps)


def per_group(values, gain):
    parts = []
    for g in range(values.shape[1] // GROUP_FEATURES):
        parts.append(rms(values[:, g * GROUP_FEATURES : (g + 1) * GROUP_FEATURES]) * gain)
    return jnp.concatenate(parts, axis=1)


def head_slice(h):
    return slice(h * GROUP_FEATURES, (h + 1) * GROUP_FEATURES)


def prefix_sum(ones, values):
    high = values.astype(bf16)
    rest = values - high.astype(f32)
    middle = rest.astype(bf16)
    low = (rest - middle.astype(f32)).astype(bf16)
    return dot(ones, jnp.concatenate([high, middle, low], axis=0))


def fused_kernel(
    tp, sp, share,
    tokens, in_gain_in, wq, wf, wi, wg, wh, wb, wc, floor_in, leak, state_gain_in, taps_in,
    group_gain_in, out_state, out_conv, result,
    in_gain, floor, state_gain, taps, group_gain, small_sem,
    normed_all, w_scan, w_conv, w_read, cums, key_mid, value_all, olds, offsets,
    pad, state, offset, read, qdev, gate, conv_all, mix_all, columns, acc_all,
    sent_state, peer_state, sent_total, totals,
    rim, tail, head_conv, head_gate, incoming,
    tok_sem, leak_sem, w_sem, own_sem,
    pair_send, pair_recv, piece_send, piece_recv, mate_send,
    blk_send, fwd_send, conv_recv, mix_first, mix_recv, l1_send, l1_recv, l2_send, l2_recv, rim_send, rim_recv,
    ready, rim_ready, twin_ready, mate_ready,
):
    me, place = lax.axis_index("tp"), lax.axis_index("sp")
    partner = me + 1 - 2 * lax.rem(me, 2)
    chips = tp // 2
    chip = lax.div(me, 2)
    core = lax.rem(me, 2)
    count, feats = normed_all.shape
    width = value_all.shape[1]
    channels = pad.shape[1]
    rows = ROWS
    nb, mix_nb = count // rows, count // MIX_ROWS
    ncols = result.shape[1]
    heads = state.shape[0]
    piece = width // share
    mine = lax.rem(place, share)
    twin = place + 1 - 2 * lax.rem(place, 2)
    across = share // 2
    step = across - share * lax.div(mine, across)
    mate, mates_piece = place + step, mine + step
    member = lax.rem(place, 2)
    pair = lax.div(place, 2)
    pairs = sp // 2
    before, after = lax.rem(place + sp - 1, sp), lax.rem(place + 1, sp)
    held = (conv_all, mix_all)
    outs = (out_conv, out_state)

    def block(t):
        if isinstance(t, int):
            return pl.ds(t * rows, rows)
        return pl.ds(pl.multiple_of(t * rows, rows), rows)

    def mix_block(t):
        return pl.ds(pl.multiple_of(t * MIX_ROWS, MIX_ROWS), MIX_ROWS)

    def token_copy(t):
        return pltpu.make_async_copy(tokens.at[block(t)], normed_all.at[block(t)], tok_sem.at[t])

    def leak_copy(t):
        at = block(0) if t == 0 else pl.ds(rows, count - rows)
        return pltpu.make_async_copy(leak.at[at], cums.at[at], leak_sem.at[t])

    weights = ((wf, 0, 0), (wi, 0, 1), (wc, 1, 0), (wh, 1, 1), (wb, 1, 2), (wq, 2, 0), (wg, 2, 1))

    phases = [w_scan, w_conv, w_read]

    def weight_copy(n):
        src, phase, slot = weights[n]
        dst = phases[phase]
        return pltpu.make_async_copy(
            src, dst.at[:, slot * width : (slot + 1) * width], w_sem.at[phase]
        )

    def weight_wait(phase):
        dst = phases[phase]
        pltpu.make_async_copy(dst, dst, w_sem.at[phase]).wait()

    def cols_of(device):
        return pl.ds(pl.multiple_of(device * ncols, ncols), ncols)

    def piece_rows(g):
        return pl.ds(pl.multiple_of(g * piece, piece), piece)

    def own_columns(kind):
        return pltpu.make_async_copy(
            outs[kind].at[:, cols_of(me)], columns.at[kind, me], own_sem.at[0]
        )

    def pair_columns(kind, origin):
        return pltpu.make_async_remote_copy(
            outs[kind].at[:, cols_of(partner)], columns.at[kind, origin],
            pair_send.at[0], pair_recv.at[0], device_id={"tp": partner},
        )

    def far(k, c):
        return lax.rem(chip + k, chips) * 2 + c

    def piece_out(kind, k, c):
        target = far(k, c)
        return pltpu.make_async_remote_copy(
            outs[kind].at[piece_rows(mine), cols_of(target)],
            columns.at[kind, me, piece_rows(mine)],
            piece_send.at[kind, k - 1, c], piece_recv.at[kind, chips - k - 1, core, 0],
            device_id={"tp": target},
        )

    def piece_in(kind, k, c, n):
        size = (piece, piece, 2 * piece)[n]
        ref = columns.at[kind, me, 0:size]
        return pltpu.make_async_copy(ref, ref, piece_recv.at[kind, k - 1, c, n])

    def pass_on(kind, k, c, n):
        g, to = ((mine, mate), (mine, twin), (mates_piece, twin))[n]
        ref = columns.at[kind, far(k, c), piece_rows(g)]
        return pltpu.make_async_remote_copy(
            ref, ref, mate_send.at[kind, k - 1, c],
            piece_recv.at[kind, k - 1, c, (1, 2, 2)[n]], device_id={"sp": to},
        )

    def pass_own(kind):
        for k, c in far_devices:
            piece_in(kind, k, c, 0).wait()
            pass_on(kind, k, c, 0).start()
            pass_on(kind, k, c, 1).start()

    def pass_mates(kind):
        for k, c in far_devices:
            piece_in(kind, k, c, 1).wait()
            pass_on(kind, k, c, 2).start()

    far_devices = [(k, c) for k in range(1, chips) for c in range(2)]

    def span(kind, t):
        if kind == CONV and isinstance(t, int):
            if t == 0:
                return pl.ds(HEAD, rows - HEAD)
            if t == nb:
                return pl.ds(0, HEAD)
        return mix_block(t) if kind == MIX else block(t)

    def recv_sem(kind, slot, t):
        return conv_recv.at[slot] if kind == CONV or slot == 0 else mix_recv.at[slot - 1, t]

    def first_recv(kind):
        return (conv_recv if kind == CONV else mix_first).at[0]

    def own_copies(kind, t):
        ref = held[kind].at[me, span(kind, t)]
        out = []
        for k in range(1, chips):
            out.append(pltpu.make_async_remote_copy(
                ref, ref, blk_send.at[kind, k], recv_sem(kind, chips - k, t),
                device_id={"tp": far(k, core)},
            ))
        out.append(pltpu.make_async_remote_copy(
            ref, ref, blk_send.at[kind, 0], first_recv(kind), device_id={"tp": partner}
        ))
        return out

    def relays(kind, t):
        out = []
        for k in range(1, chips):
            ref = held[kind].at[far(k, core)]
            if kind == MIX:
                ref = ref.at[mix_block(t)]
            out.append(pltpu.make_async_remote_copy(
                ref, ref, fwd_send.at[kind, k - 1], recv_sem(kind, chips - 1 + k, t),
                device_id={"tp": partner},
            ))
        return out

    def start(copies):
        for copy in copies:
            copy.start()

    def landed(kind, slot, t):
        ref = held[kind].at[me]
        if kind == MIX:
            ref = ref.at[mix_block(t)]
        pltpu.make_async_copy(ref, ref, recv_sem(kind, slot, t)).wait()

    def relay(kind, t):
        for k, copy in enumerate(relays(kind, t)):
            landed(kind, k + 1, t)
            copy.start()

    def first_landed(kind):
        ref = held[kind].at[me]
        pltpu.make_async_copy(ref, ref, first_recv(kind)).wait()

    def sent(kind):
        ref = held[kind].at[me]
        for k in range(chips):
            pltpu.make_async_copy(ref, ref, blk_send.at[kind, k]).wait()

    def passed_on(kind):
        ref = held[kind].at[me]
        for k in range(1, chips):
            pltpu.make_async_copy(ref, ref, fwd_send.at[kind, k - 1]).wait()

    twin_copy = pltpu.make_async_remote_copy(
        sent_state, peer_state, l1_send.at[0], l1_recv.at[0], device_id={"sp": twin}
    )

    def total_copy(k, source):
        return pltpu.make_async_remote_copy(
            sent_total, totals.at[source], l2_send.at[k - 1], l2_recv.at[source],
            device_id={"sp": lax.rem(place + 2 * k, sp)},
        )

    def put_decay(ref, decay):
        high = decay.astype(bf16)
        low = (decay - high.astype(f32)).astype(bf16)
        for h in range(heads):
            s = head_slice(h)
            both = jnp.concatenate([high[:, s], low[:, s]], axis=0)
            both = jnp.concatenate([both] * (EXTRA // 2), axis=0)
            ref[h, GROUP_FEATURES:, :] = both

    def decay_of(rows_of):
        both = rows_of.astype(f32)
        return both[0:1] + both[1:2]

    rim_copy = pltpu.make_async_remote_copy(
        tail, rim, rim_send.at[0], rim_recv.at[0], device_id={"sp": after}
    )

    small = ((in_gain_in, in_gain), (floor_in, floor), (state_gain_in, state_gain),
             (taps_in, taps), (group_gain_in, group_gain))

    def small_copy(n):
        return pltpu.make_async_copy(small[n][0], small[n][1], small_sem.at[n])

    small_copy(0).start()
    token_copy(0).start()
    weight_copy(0).start()
    weight_copy(1).start()
    small_copy(1).start()
    leak_copy(0).start()
    if nb > 1:
        token_copy(1).start()
        leak_copy(1).start()
    barrier = pltpu.get_barrier_semaphore()
    for k in range(1, tp):
        pl.semaphore_signal(barrier, inc=1, device_id={"tp": lax.rem(me + k, tp)})
    for to, low in ((twin, member == 0), (mate, step > 0)):
        @pl.when(low)
        def _():
            pl.semaphore_signal(barrier, inc=1, device_id={"sp": to})

    for k in range(1, pairs):
        @pl.when(pair + k < pairs)
        def _():
            pl.semaphore_signal(barrier, inc=1, device_id={"sp": lax.rem(place + 2 * k, sp)})
    follows = jnp.logical_and(member == 0, pair > 0)
    leads = jnp.logical_and(member == 1, pair < pairs - 1)

    @pl.when(leads)
    def _():
        pl.semaphore_signal(barrier, inc=1, device_id={"sp": after})

    lower = pair + member + jnp.where(step > 0, 0, 1) + jnp.where(follows, 1, 0)
    pl.semaphore_wait(barrier, tp - 1 + lower)

    @pl.when(member == 1)
    def _():
        pl.semaphore_signal(twin_ready, inc=1, device_id={"sp": twin})

    @pl.when(step < 0)
    def _():
        pl.semaphore_signal(mate_ready, inc=1, device_id={"sp": mate})

    for k in range(1, pairs):
        @pl.when(pair >= k)
        def _():
            pl.semaphore_signal(ready, inc=1, device_id={"sp": lax.rem(place + sp - 2 * k, sp)})

    @pl.when(follows)
    def _():
        pl.semaphore_signal(rim_ready, inc=1, device_id={"sp": before})
    for kind in (CONV, MIX):
        for k, c in far_devices:
            piece_out(kind, k, c).start()
    for t in range(2, nb):
        token_copy(t).start()
    for n in (2, 3, 4):
        small_copy(n).start()
    for kind in (CONV, MIX):
        pair_columns(kind, me).start()
        own_columns(kind).start()

    state[...] = jnp.zeros_like(state)
    offset[...] = jnp.zeros_like(offset)
    pad[0:HALO, :] = jnp.zeros((HALO, channels), f32)

    r = lax.broadcasted_iota(jnp.int32, (CHUNK, CHUNK), 0)
    c = lax.broadcasted_iota(jnp.int32, (CHUNK, CHUNK), 1)
    causal = r >= c
    ones = jnp.concatenate([causal.astype(f32)] * 3, axis=1).astype(bf16)

    def arrive(t):
        token_copy(t).wait()
        if t < 2:
            leak_copy(t).wait()

    def norm(t):
        arrive(t)
        normalize(t)

    def normalize(t):
        at = block(t)
        normed_all[at, :] = (rms(normed_all[at, :].astype(f32)) * in_gain[...]).astype(bf16)

    def scan_product(t):
        return dot(normed_all[block(t), :], w_scan[...])

    def scan_block(t, both):
        at = block(t)
        x = both[:, :width].astype(bf16).astype(f32)
        value = both[:, width:].astype(bf16)
        value_all[at, :] = value
        key = (1.0 - floor[...]) * jax.nn.sigmoid(-x)
        logf = jnp.log(1.0 - key) + cums[at, :]
        for b in range(rows // CHUNK):
            lo, hi = b * CHUNK, (b + 1) * CHUNK
            where = pl.ds(t * rows + lo, CHUNK)
            number = t * (rows // CHUNK) + b
            cum = prefix_sum(ones, logf[lo:hi])
            mid = cum[CHUNK // 2 - 1 : CHUNK // 2]
            last = cum[CHUNK - 1 : CHUNK]
            k_mid = key[lo:hi] * jnp.exp(mid - cum)
            k_end = (k_mid * jnp.exp(last - mid)).astype(bf16)
            cums[where, :] = cum
            key_mid[where, :] = k_mid.astype(bf16)
            offsets[number] = offset[...]
            for h in range(heads):
                s = head_slice(h)
                old = state[h]
                olds[number, h] = old.astype(bf16)
                state[h] = old * jnp.exp(last[:, s]) + dot(
                    value[lo:hi, s], k_end[:, s], ((0,), (0,))
                )
            offset[...] += last

    small_copy(0).wait()
    norm(0)
    small_copy(1).wait()
    weight_wait(0)
    for n in range(2, 7):
        weight_copy(n).start()
    product = scan_product(0)
    if nb > 1:
        norm(1)
    for t in range(nb):
        if t + 2 < nb:
            arrive(t + 2)
        if t + 1 < nb:
            later = scan_product(t + 1)
        if t + 2 < nb:
            normalize(t + 2)
        scan_block(t, product)
        product = later
    sent_state[:, :GROUP_FEATURES, :] = state[...].astype(bf16)
    put_decay(sent_state, jnp.exp(offset[0:1, :]))

    @pl.when(member == 0)
    def _():
        pl.semaphore_wait(twin_ready, 1)

    twin_copy.start()

    @pl.when(step > 0)
    def _():
        pl.semaphore_wait(mate_ready, 1)

    pass_own(CONV)

    weight_wait(1)
    for n in (2, 3, 4):
        small_copy(n).wait()
    w_taps = taps[...].astype(f32)

    def conv_product(t):
        return dot(normed_all[block(t), :], w_conv[...])

    def conv_block(t, three):
        at = block(t)
        first = three[:, :channels].astype(bf16).astype(f32)
        second = three[:, channels : 2 * channels].astype(bf16).astype(f32)
        proj_b = three[:, 2 * channels :].astype(bf16).astype(f32)
        conv_in = (first * second).astype(bf16).astype(f32)
        pad[HALO : HALO + rows, :] = conv_in
        total = w_taps[TAPS - 1 : TAPS] * conv_in
        for j in range(TAPS - 1):
            lo = HALO - (TAPS - 1) + j
            total += w_taps[j : j + 1] * pad[lo : lo + rows, :]
        conv_all[me, at, :] = per_group(proj_b * total, group_gain[...]).astype(bf16)

        @pl.when(t == 0)
        def _():
            head_conv[...] = conv_in[:HALO]
            head_gate[...] = proj_b[:HALO]
            start(own_copies(CONV, 0))

        @pl.when(t > 0)
        def _():
            start(own_copies(CONV, t))

        pad[0:HALO, :] = conv_in[rows - HALO :]

        @pl.when(t == nb - 1)
        def _():
            tail[...] = conv_in[rows - HALO :]

            @pl.when(leads)
            def _():
                pl.semaphore_wait(rim_ready, 1)

            @pl.when(place < sp - 1)
            def _():
                rim_copy.start()

            pass_mates(CONV)

        @pl.when(t == min(2, nb - 1))
        def _():
            twin_copy.wait_recv()
            decays = []
            for h in range(heads):
                s = head_slice(h)
                own, other = state[h], peer_state[h, :GROUP_FEATURES, :].astype(f32)
                own_decay = jnp.exp(offset[0:1, s])
                peer_decay = decay_of(peer_state[h, GROUP_FEATURES:, :])
                early = jnp.where(member == 0, own, other)
                late = jnp.where(member == 0, other, own)
                decay = jnp.where(member == 0, peer_decay, own_decay)
                sent_total[h, :GROUP_FEATURES, :] = (early * decay + late).astype(bf16)
                decays.append(own_decay * peer_decay)
            put_decay(sent_total, jnp.concatenate(decays, axis=1))

            @pl.when(pair < pairs - 1)
            def _():
                pl.semaphore_wait(ready, pairs - 1 - pair)

            for k in range(1, pairs):
                @pl.when(pair + k < pairs)
                def _():
                    total_copy(k, pair).start()

    product = conv_product(0)
    for t in range(nb):
        if t + 1 < nb:
            later = conv_product(t + 1)
        conv_block(t, product)
        product = later

    weight_wait(2)

    def read_product(t):
        return dot(normed_all[block(t), :], w_read[...])

    def read_block(t, both):
        at = block(t)
        query = jax.nn.silu(both[:, :width].astype(bf16).astype(f32))
        outgate = jax.nn.silu(both[:, width:].astype(bf16).astype(f32))
        for h in range(heads):
            s = head_slice(h)
            gate[at, s] = outgate[:, s] * state_gain[...]
        for b in range(rows // CHUNK):
            lo, hi = b * CHUNK, (b + 1) * CHUNK
            where = pl.ds(t * rows + lo, CHUNK)
            number = t * (rows // CHUNK) + b
            cum = cums[where, :]
            mid = cum[CHUNK // 2 - 1 : CHUNK // 2]
            q_mid = query[lo:hi] * jnp.exp(cum - mid)
            q_all = q_mid * jnp.exp(mid)
            qdev[where, :] = (q_all * jnp.exp(offsets[number, 0:1, :])).astype(bf16)
            q_mid, q_all = q_mid.astype(bf16), q_all.astype(bf16)
            for h in range(heads):
                s = head_slice(h)
                scores = dot(q_mid[:, s], key_mid[where, s], ((1,), (1,)))
                scores = jnp.where(causal, scores, 0.0).astype(bf16)
                read[where, s] = dot(scores, value_all[where, s]) + dot(
                    q_all[:, s], olds[number, h], ((1,), (1,))
                )

        @pl.when(t == nb - 1)
        def _():
            @pl.when(place == 0)
            def _():
                rim[...] = jnp.zeros_like(rim)

            @pl.when(place > 0)
            def _():
                rim_copy.wait_recv()

            ext = jnp.concatenate([rim[...], head_conv[...]], axis=0)
            fixed = w_taps[TAPS - 1 : TAPS] * head_conv[...]
            for j in range(TAPS - 1):
                lo = HALO - (TAPS - 1) + j
                fixed += w_taps[j : j + 1] * ext[lo : lo + HALO]
            fixed = per_group(head_gate[...] * fixed, group_gain[...])
            conv_all[me, 0:HALO, :] = fixed.astype(bf16)
            start(own_copies(CONV, nb))

    product = read_product(0)
    for t in range(nb):
        if t + 1 < nb:
            later = read_product(t + 1)
        read_block(t, product)
        product = later

    for k in range(1, pairs):
        @pl.when(pair >= k)
        def _():
            total_copy(k, pair - k).wait_recv()
    incoming[...] = jnp.zeros_like(incoming)

    def hop(p, _):
        for h in range(heads):
            decay = decay_of(totals[p, h, GROUP_FEATURES:, :])
            incoming[h] = incoming[h] * decay + totals[p, h, :GROUP_FEATURES, :].astype(f32)
        return 0

    lax.fori_loop(0, pair, hop, 0)
    for h in range(heads):
        decay = decay_of(peer_state[h, GROUP_FEATURES:, :])
        through = incoming[h] * decay + peer_state[h, :GROUP_FEATURES, :].astype(f32)
        incoming[h] = jnp.where(member == 0, incoming[h], through)

    def merge(t, _):
        at = block(t)
        for h in range(heads):
            s = head_slice(h)
            whole = read[at, s] + dot(qdev[at, s], incoming[h].astype(bf16), ((1,), (1,)))
            mix_all[me, at, s] = (rms(whole) * gate[at, s]).astype(bf16)
        for n in range(rows // MIX_ROWS):
            start(own_copies(MIX, t * (rows // MIX_ROWS) + n))
        return 0

    lax.fori_loop(0, nb, merge, 0)
    pass_own(MIX)

    mine_both, pair_both = columns.at[:, me], columns.at[:, partner]
    pltpu.make_async_copy(mine_both, mine_both, own_sem.at[0]).wait()
    pltpu.make_async_copy(pair_both, pair_both, pair_recv.at[0]).wait()

    def near(kind, t):
        out = dot(held[kind][me, block(t), :], columns[kind, me])
        return out + dot(held[kind][partner, block(t), :], columns[kind, partner])

    def near_conv(t, _):
        acc_all[block(t), :] = near(CONV, t)
        return 0

    first_landed(CONV)
    lax.fori_loop(0, nb, near_conv, 0)


    def near_mix(t, _):
        acc_all[block(t), :] += near(MIX, t)
        return 0

    first_landed(MIX)
    lax.fori_loop(0, nb, near_mix, 0)

    pass_mates(MIX)

    relay(CONV, 0)
    for kind in (CONV, MIX):
        for k, c in far_devices:
            piece_in(kind, k, c, 2).wait()
    for k in range(1, chips):
        landed(CONV, chips - 1 + k, 0)

    def far_conv(t, _):
        acc = acc_all[block(t), :]
        for k, c in far_devices:
            origin = far(k, c)
            acc += dot(conv_all[origin, block(t), :], columns[CONV, origin])
        acc_all[block(t), :] = acc
        return 0

    lax.fori_loop(0, nb, far_conv, 0)

    sent(CONV)
    passed_on(CONV)
    for kind in (CONV, MIX):
        for k, c in far_devices:
            piece_out(kind, k, c).wait_send()
            passed = columns.at[kind, me, 0 : 3 * piece]
            pltpu.make_async_copy(passed, passed, mate_send.at[kind, k - 1, c]).wait()
    pltpu.make_async_copy(mine_both, mine_both, pair_send.at[0]).wait()

    @pl.when(place < sp - 1)
    def _():
        rim_copy.wait_send()

    twin_copy.wait_send()
    for k in range(1, pairs):
        @pl.when(pair + k < pairs)
        def _():
            total_copy(k, pair).wait_send()

    def finish(t, _):
        @pl.when(t + LAG < mix_nb)
        def _():
            relay(MIX, t + LAG)

        for k in range(1, chips):
            landed(MIX, chips - 1 + k, t)
        at = mix_block(t)
        acc = acc_all[at, :]
        for k, c in far_devices:
            origin = far(k, c)
            acc += dot(mix_all[origin, at, :], columns[MIX, origin])
        result[at, :] = acc.astype(bf16)
        return 0

    for t in range(min(LAG, mix_nb)):
        relay(MIX, t)
    lax.fori_loop(0, mix_nb, finish, 0)

    sent(MIX)
    passed_on(MIX)


def body(
    tokens, in_gain, w_query, w_forget, w_input, w_outgate, w_conv_h, w_conv_b, w_conv_c,
    forget_floor, forget_leak, state_gain, conv_taps, group_gain, out_state, out_conv,
):
    count, feats = tokens.shape
    width, channels = w_query.shape[1], w_conv_h.shape[1]
    heads = width // GROUP_FEATURES
    tp, sp = lax.axis_size("tp"), lax.axis_size("sp")
    ncols, nb, chips = out_state.shape[1] // tp, count // ROWS, tp // 2
    share = min(SHARE, sp)
    chunks, pairs = count // CHUNK, sp // 2

    hbm = pl.BlockSpec(memory_space=pltpu.HBM)
    vmem = pl.BlockSpec(memory_space=pltpu.VMEM)
    sems = pltpu.SemaphoreType.DMA
    square = (heads, GROUP_FEATURES, GROUP_FEATURES)
    longer = (heads, GROUP_FEATURES + EXTRA, GROUP_FEATURES)
    return pl.pallas_call(
        functools.partial(fused_kernel, tp, sp, share),
        in_specs=[hbm] * 16,
        out_specs=vmem,
        out_shape=pltpu.VMEM((count, ncols), bf16),
        scratch_shapes=[
            pltpu.VMEM((1, feats), f32),
            pltpu.VMEM((1, width), f32),
            pltpu.VMEM((1, GROUP_FEATURES), f32),
            pltpu.VMEM((TAPS, channels), bf16),
            pltpu.VMEM((1, GROUP_FEATURES), f32),
            sems((5,)),
            pltpu.VMEM((count, feats), bf16),
            pltpu.VMEM((feats, 2 * width), bf16),
            pltpu.VMEM((feats, 3 * channels), bf16),
            pltpu.VMEM((feats, 2 * width), bf16),
            pltpu.VMEM((count, width), f32),
            pltpu.VMEM((count, width), bf16),
            pltpu.VMEM((count, width), bf16),
            pltpu.VMEM((chunks,) + square, bf16),
            pltpu.VMEM((chunks, HALO, width), f32),
            pltpu.VMEM((HALO + ROWS, channels), f32),
            pltpu.VMEM(square, f32),
            pltpu.VMEM((HALO, width), f32),
            pltpu.VMEM((count, width), f32),
            pltpu.VMEM((count, width), bf16),
            pltpu.VMEM((count, width), f32),
            pltpu.VMEM((tp, count, channels), bf16),
            pltpu.VMEM((tp, count, width), bf16),
            pltpu.VMEM((2, tp, width, ncols), bf16),
            pltpu.VMEM((count, ncols), f32),
            pltpu.VMEM(longer, bf16),
            pltpu.VMEM(longer, bf16),
            pltpu.VMEM(longer, bf16),
            pltpu.VMEM((pairs,) + longer, bf16),
            pltpu.VMEM((HALO, channels), f32),
            pltpu.VMEM((HALO, channels), f32),
            pltpu.VMEM((HALO, channels), f32),
            pltpu.VMEM((HALO, channels), f32),
            pltpu.VMEM(square, f32),
            sems((nb,)), sems((2,)), sems((3,)), sems((1,)),
            sems((1,)), sems((1,)), sems((2, chips - 1, 2)), sems((2, chips - 1, 2, 3)),
            sems((2, chips - 1, 2)),
            sems((2, chips)), sems((2, chips - 1)), sems((2 * chips - 1,)), sems((1,)),
            sems((2 * chips - 2, count // MIX_ROWS)),
            sems((1,)), sems((1,)), sems((pairs - 1,)), sems((pairs,)), sems((1,)), sems((1,)),
        ] + [pltpu.SemaphoreType.REGULAR] * 4,
        compiler_params=pltpu.CompilerParams(
            vmem_limit_bytes=56 * 2**20, collective_id=0, has_side_effects=True
        ),
    )(
        tokens, in_gain[None], w_query, w_forget, w_input, w_outgate, w_conv_h, w_conv_b, w_conv_c,
        forget_floor[None], forget_leak, state_gain[None], conv_taps, group_gain[None],
        out_state, out_conv,
    )


def solution(mesh):
    cols, rows = P(None, "tp"), P("tp", None)
    in_specs = (
        P("sp", None), P(), cols, cols, cols, cols, cols, cols, cols,
        P("tp"), P("sp", "tp"), P(), cols, P(), rows, rows,
    )
    return jax.shard_map(
        body, mesh=mesh, in_specs=in_specs, out_specs=P("sp", "tp"), check_vma=False
    )
```

time: 40.9 us -> 37.9 us (0.927)
  Pallas kernels: 39.8 us -> 36.8 us
    pallas_call x1, Pallas kernels: 39.8 us -> 36.8 us  [body(): pl.pallas_call(functools.partial(fused_kernel, tp, sp, share), in_specs=[...]
where the time goes in v3:
time: 37.9 us; the launch traced here: 37.8 us
  Pallas kernels  36.8 us (97%)
  local copies, waits for them, and re-layouts  0.97 us (3%)
    pallas_call x1, Pallas kernels, body(): pl.pallas_call(functools.partial(fused_kernel, tp, sp, share), in_specs=[...  36.8 us
    unnamed x1, local copies, waits for them, and re-layouts  0.97 us

profile of v3, /device:TPU:1, one launch (start us, length us, event | category | flops | bytes accessed | tf_op | source)
XLA Modules:
  0.0 37.8 jit_solution(5535359532805090809)
XLA Ops:
  0.0 36.8 %shard_map.154 = bf16[1024,512]{1,0:T(8,128)(2,1)S(1)} custom-call(bf16[1024,2048]{1,0:T(8,128)(2,1)} %tokens.1, f32[1,2048]{1,0:T(1,128)} %bitcast.4, bf16[2048,256]{1,0:T(8,128)(2,1)} %wq.1, bf16[2048,256]{1,0:T(8,128)(2,1)} %wf.1, bf16[2048,256]{1,0:T(8,128)(2,1)} %wi.1, bf16[2048,256]{1,0:T(8,128)(2,1)} %wg.1, bf16[2048,256]{1,0:T(8,128)(2,1)} %wh.1, ...), custom_call_target="tpu_custom_call" | custom-call | tf_op jit(solution)/shard_map/pallas_call | solution.py:690
  36.8 1.0 %copy.18 = bf16[1024,512]{1,0:T(8,128)(2,1)} copy(bf16[1024,512]{1,0:T(8,128)(2,1)S(1)} %shard_map.154) | data formatting | bytes 2097152

commit v4 on v3

--- a/solution.py
+++ b/solution.py
@@ -106,6 +106,7 @@
         return pltpu.make_async_copy(leak.at[at], cums.at[at], leak_sem.at[t])
 
     weights = ((wf, 0, 0), (wi, 0, 1), (wc, 1, 0), (wh, 1, 1), (wb, 1, 2), (wq, 2, 0), (wg, 2, 1))
+    weight_sems = (0, 0, 1, 2, 3, 4, 4)
 
     phases = [w_scan, w_conv, w_read]
 
@@ -113,12 +114,12 @@
         src, phase, slot = weights[n]
         dst = phases[phase]
         return pltpu.make_async_copy(
-            src, dst.at[:, slot * width : (slot + 1) * width], w_sem.at[phase]
+            src, dst.at[:, slot * width : (slot + 1) * width], w_sem.at[weight_sems[n]]
         )
 
     def weight_wait(phase):
         dst = phases[phase]
-        pltpu.make_async_copy(dst, dst, w_sem.at[phase]).wait()
+        pltpu.make_async_copy(dst, dst, w_sem.at[weight_sems[2 * phase + phase // 2]]).wait()
 
     def cols_of(device):
         return pl.ds(pl.multiple_of(device * ncols, ncols), ncols)
@@ -162,11 +163,12 @@
             piece_recv.at[kind, k - 1, c, (1, 2, 2)[n]], device_id={"sp": to},
         )
 
-    def pass_own(kind):
+    def pass_own(kind, wait, which):
         for k, c in far_devices:
-            piece_in(kind, k, c, 0).wait()
-            pass_on(kind, k, c, 0).start()
-            pass_on(kind, k, c, 1).start()
+            if wait:
+                piece_in(kind, k, c, 0).wait()
+            for n in which:
+                pass_on(kind, k, c, n).start()
 
     def pass_mates(kind):
         for k, c in far_devices:
@@ -243,24 +245,23 @@
         for k in range(1, chips):
             pltpu.make_async_copy(ref, ref, fwd_send.at[kind, k - 1]).wait()
 
-    twin_copy = pltpu.make_async_remote_copy(
-        sent_state, peer_state, l1_send.at[0], l1_recv.at[0], device_id={"sp": twin}
-    )
-
-    def total_copy(k, source):
+    def twin_copy(h):
         return pltpu.make_async_remote_copy(
-            sent_total, totals.at[source], l2_send.at[k - 1], l2_recv.at[source],
+            sent_state.at[h], peer_state.at[h], l1_send.at[h], l1_recv.at[h],
+            device_id={"sp": twin},
+        )
+
+    def total_copy(k, source, h):
+        return pltpu.make_async_remote_copy(
+            sent_total.at[h], totals.at[source, h], l2_send.at[h, k - 1], l2_recv.at[h, source],
             device_id={"sp": lax.rem(place + 2 * k, sp)},
         )
 
-    def put_decay(ref, decay):
+    def put_decay(ref, h, decay):
         high = decay.astype(bf16)
         low = (decay - high.astype(f32)).astype(bf16)
-        for h in range(heads):
-            s = head_slice(h)
-            both = jnp.concatenate([high[:, s], low[:, s]], axis=0)
-            both = jnp.concatenate([both] * (EXTRA // 2), axis=0)
-            ref[h, GROUP_FEATURES:, :] = both
+        both = jnp.concatenate([high, low], axis=0)
+        ref[h, GROUP_FEATURES:, :] = jnp.concatenate([both] * (EXTRA // 2), axis=0)
 
     def decay_of(rows_of):
         both = rows_of.astype(f32)
@@ -387,6 +388,81 @@
                 )
             offset[...] += last
 
+    def conv_third(n):
+        return dot(normed_all[block(0), :], w_conv[:, n * channels : (n + 1) * channels])
+
+
+    def conv_product(t):
+        return dot(normed_all[block(t), :], w_conv[...])
+
+    def conv_block(t, three):
+        at = block(t)
+        first = three[:, :channels].astype(bf16).astype(f32)
+        second = three[:, channels : 2 * channels].astype(bf16).astype(f32)
+        proj_b = three[:, 2 * channels :].astype(bf16).astype(f32)
+        conv_in = (first * second).astype(bf16).astype(f32)
+        w_taps = taps[...].astype(f32)
+        pad[HALO : HALO + rows, :] = conv_in
+        total = w_taps[TAPS - 1 : TAPS] * conv_in
+        for j in range(TAPS - 1):
+            lo = HALO - (TAPS - 1) + j
+            total += w_taps[j : j + 1] * pad[lo : lo + rows, :]
+        conv_all[me, at, :] = per_group(proj_b * total, group_gain[...]).astype(bf16)
+
+        @pl.when(t == 0)
+        def _():
+            head_conv[...] = conv_in[:HALO]
+            head_gate[...] = proj_b[:HALO]
+            start(own_copies(CONV, 0))
+
+        @pl.when(t > 0)
+        def _():
+            start(own_copies(CONV, t))
+
+        pad[0:HALO, :] = conv_in[rows - HALO :]
+
+        @pl.when(t == nb - 1)
+        def _():
+            tail[...] = conv_in[rows - HALO :]
+
+            @pl.when(leads)
+            def _():
+                pl.semaphore_wait(rim_ready, 1)
+
+            @pl.when(place < sp - 1)
+            def _():
+                rim_copy.start()
+
+            pass_own(MIX, True, (1,))
+
+            @pl.when(step < 0)
+            def _():
+                pass_own(MIX, False, (0,))
+
+
+        @pl.when(t == nb - 1)
+        def _():
+            @pl.when(pair < pairs - 1)
+            def _():
+                pl.semaphore_wait(ready, pairs - 1 - pair)
+
+            for h in range(heads):
+                s = head_slice(h)
+                twin_copy(h).wait_recv()
+                own, other = state[h], peer_state[h, :GROUP_FEATURES, :].astype(f32)
+                own_decay = jnp.exp(offset[0:1, s])
+                peer_decay = decay_of(peer_state[h, GROUP_FEATURES:, :])
+                early = jnp.where(member == 0, own, other)
+                late = jnp.where(member == 0, other, own)
+                decay = jnp.where(member == 0, peer_decay, own_decay)
+                sent_total[h, :GROUP_FEATURES, :] = (early * decay + late).astype(bf16)
+                put_decay(sent_total, h, own_decay * peer_decay)
+                for k in range(1, pairs):
+                    @pl.when(pair + k < pairs)
+                    def _():
+                        total_copy(k, pair, h).start()
+
+    conv_thirds = []
     small_copy(0).wait()
     norm(0)
     small_copy(1).wait()
@@ -399,101 +475,41 @@
     for t in range(nb):
         if t + 2 < nb:
             arrive(t + 2)
+        thirds = [n for n in range(3) if t == max(nb - 3 + min(n, 1), 0)]
+        for n in thirds:
+            weight_copy(2 + n).wait()
         if t + 1 < nb:
             later = scan_product(t + 1)
+        for n in thirds:
+            conv_thirds.append(conv_third(n))
         if t + 2 < nb:
             normalize(t + 2)
+        if t == nb - 1:
+            for n in (2, 3, 4):
+                small_copy(n).wait()
+            conv_block(0, jnp.concatenate(conv_thirds, axis=1))
         scan_block(t, product)
         product = later
     sent_state[:, :GROUP_FEATURES, :] = state[...].astype(bf16)
-    put_decay(sent_state, jnp.exp(offset[0:1, :]))
+    for h in range(heads):
+        put_decay(sent_state, h, jnp.exp(offset[0:1, head_slice(h)]))
 
     @pl.when(member == 0)
     def _():
         pl.semaphore_wait(twin_ready, 1)
 
-    twin_copy.start()
+    for h in range(heads):
+        twin_copy(h).start()
 
     @pl.when(step > 0)
     def _():
         pl.semaphore_wait(mate_ready, 1)
 
-    pass_own(CONV)
-
-    weight_wait(1)
-    for n in (2, 3, 4):
-        small_copy(n).wait()
-    w_taps = taps[...].astype(f32)
-
-    def conv_product(t):
-        return dot(normed_all[block(t), :], w_conv[...])
-
-    def conv_block(t, three):
-        at = block(t)
-        first = three[:, :channels].astype(bf16).astype(f32)
-        second = three[:, channels : 2 * channels].astype(bf16).astype(f32)
-        proj_b = three[:, 2 * channels :].astype(bf16).astype(f32)
-        conv_in = (first * second).astype(bf16).astype(f32)
-        pad[HALO : HALO + rows, :] = conv_in
-        total = w_taps[TAPS - 1 : TAPS] * conv_in
-        for j in range(TAPS - 1):
-            lo = HALO - (TAPS - 1) + j
-            total += w_taps[j : j + 1] * pad[lo : lo + rows, :]
-        conv_all[me, at, :] = per_group(proj_b * total, group_gain[...]).astype(bf16)
-
-        @pl.when(t == 0)
-        def _():
-            head_conv[...] = conv_in[:HALO]
-            head_gate[...] = proj_b[:HALO]
-            start(own_copies(CONV, 0))
-
-        @pl.when(t > 0)
-        def _():
-            start(own_copies(CONV, t))
-
-        pad[0:HALO, :] = conv_in[rows - HALO :]
-
-        @pl.when(t == nb - 1)
-        def _():
-            tail[...] = conv_in[rows - HALO :]
-
-            @pl.when(leads)
-            def _():
-                pl.semaphore_wait(rim_ready, 1)
-
-            @pl.when(place < sp - 1)
-            def _():
-                rim_copy.start()
-
-            pass_mates(CONV)
-
-        @pl.when(t == min(2, nb - 1))
-        def _():
-            twin_copy.wait_recv()
-            decays = []
-            for h in range(heads):
-                s = head_slice(h)
-                own, other = state[h], peer_state[h, :GROUP_FEATURES, :].astype(f32)
-                own_decay = jnp.exp(offset[0:1, s])
-                peer_decay = decay_of(peer_state[h, GROUP_FEATURES:, :])
-                early = jnp.where(member == 0, own, other)
-                late = jnp.where(member == 0, other, own)
-                decay = jnp.where(member == 0, peer_decay, own_decay)
-                sent_total[h, :GROUP_FEATURES, :] = (early * decay + late).astype(bf16)
-                decays.append(own_decay * peer_decay)
-            put_decay(sent_total, jnp.concatenate(decays, axis=1))
-
-            @pl.when(pair < pairs - 1)
-            def _():
-                pl.semaphore_wait(ready, pairs - 1 - pair)
-
-            for k in range(1, pairs):
-                @pl.when(pair + k < pairs)
-                def _():
-                    total_copy(k, pair).start()
-
-    product = conv_product(0)
-    for t in range(nb):
+    pass_own(CONV, True, (0, 1))
+
+    if nb > 1:
+        product = conv_product(1)
+    for t in range(1, nb):
         if t + 1 < nb:
             later = conv_product(t + 1)
         conv_block(t, product)
@@ -529,6 +545,9 @@
                     q_all[:, s], olds[number, h], ((1,), (1,))
                 )
 
+        if t == nb // 2:
+            pass_mates(CONV)
+
         @pl.when(t == nb - 1)
         def _():
             @pl.when(place == 0)
@@ -540,6 +559,7 @@
                 rim_copy.wait_recv()
 
             ext = jnp.concatenate([rim[...], head_conv[...]], axis=0)
+            w_taps = taps[...].astype(f32)
             fixed = w_taps[TAPS - 1 : TAPS] * head_conv[...]
             for j in range(TAPS - 1):
                 lo = HALO - (TAPS - 1) + j
@@ -548,6 +568,12 @@
             conv_all[me, 0:HALO, :] = fixed.astype(bf16)
             start(own_copies(CONV, nb))
 
+            @pl.when(step > 0)
+            def _():
+                pass_own(MIX, False, (0,))
+                pass_mates(MIX)
+
+
     product = read_product(0)
     for t in range(nb):
         if t + 1 < nb:
@@ -558,7 +584,8 @@
     for k in range(1, pairs):
         @pl.when(pair >= k)
         def _():
-            total_copy(k, pair - k).wait_recv()
+            for h in range(heads):
+                total_copy(k, pair - k, h).wait_recv()
     incoming[...] = jnp.zeros_like(incoming)
 
     def hop(p, _):
@@ -584,7 +611,6 @@
         return 0
 
     lax.fori_loop(0, nb, merge, 0)
-    pass_own(MIX)
 
     mine_both, pair_both = columns.at[:, me], columns.at[:, partner]
     pltpu.make_async_copy(mine_both, mine_both, own_sem.at[0]).wait()
@@ -601,7 +627,6 @@
     first_landed(CONV)
     lax.fori_loop(0, nb, near_conv, 0)
 
-
     def near_mix(t, _):
         acc_all[block(t), :] += near(MIX, t)
         return 0
@@ -609,9 +634,12 @@
     first_landed(MIX)
     lax.fori_loop(0, nb, near_mix, 0)
 
-    pass_mates(MIX)
+    @pl.when(step < 0)
+    def _():
+        pass_mates(MIX)
 
     relay(CONV, 0)
+
     for kind in (CONV, MIX):
         for k, c in far_devices:
             piece_in(kind, k, c, 2).wait()
@@ -641,11 +669,13 @@
     def _():
         rim_copy.wait_send()
 
-    twin_copy.wait_send()
+    for h in range(heads):
+        twin_copy(h).wait_send()
     for k in range(1, pairs):
         @pl.when(pair + k < pairs)
         def _():
-            total_copy(k, pair).wait_send()
+            for h in range(heads):
+                total_copy(k, pair, h).wait_send()
 
     def finish(t, _):
         @pl.when(t + LAG < mix_nb)
@@ -727,12 +757,13 @@
             pltpu.VMEM((HALO, channels), f32),
             pltpu.VMEM((HALO, channels), f32),
             pltpu.VMEM(square, f32),
-            sems((nb,)), sems((2,)), sems((3,)), sems((1,)),
+            sems((nb,)), sems((2,)), sems((5,)), sems((1,)),
             sems((1,)), sems((1,)), sems((2, chips - 1, 2)), sems((2, chips - 1, 2, 3)),
             sems((2, chips - 1, 2)),
             sems((2, chips)), sems((2, chips - 1)), sems((2 * chips - 1,)), sems((1,)),
             sems((2 * chips - 2, count // MIX_ROWS)),
-            sems((1,)), sems((1,)), sems((pairs - 1,)), sems((pairs,)), sems((1,)), sems((1,)),
+            sems((heads,)), sems((heads,)), sems((heads, pairs - 1)), sems((heads, pairs)),
+            sems((1,)), sems((1,)),
         ] + [pltpu.SemaphoreType.REGULAR] * 4,
         compiler_params=pltpu.CompilerParams(
             vmem_limit_bytes=56 * 2**20, collective_id=0, has_side_effects=True

time: 37.9 us -> 37.2 us (0.982)
  Pallas kernels: 36.8 us -> 36.1 us
    pallas_call x1, Pallas kernels: 36.8 us -> 36.1 us  [body(): pl.pallas_call(functools.partial(fused_kernel, tp, sp, share), in_specs=[...]
where the time goes in v4:
time: 37.2 us; the launch traced here: 37.1 us
  Pallas kernels  36.1 us (97%)
  local copies, waits for them, and re-layouts  0.97 us (3%)
    pallas_call x1, Pallas kernels, body(): pl.pallas_call(functools.partial(fused_kernel, tp, sp, share), in_specs=[...  36.1 us
    unnamed x1, local copies, waits for them, and re-layouts  0.97 us

profile of v4, /device:TPU:1, one launch (start us, length us, event | category | flops | bytes accessed | tf_op | source)
XLA Modules:
  0.0 37.1 jit_solution(15151002703714462504)
XLA Ops:
  0.0 36.1 %shard_map.154 = bf16[1024,512]{1,0:T(8,128)(2,1)S(1)} custom-call(bf16[1024,2048]{1,0:T(8,128)(2,1)} %tokens.1, f32[1,2048]{1,0:T(1,128)} %bitcast.4, bf16[2048,256]{1,0:T(8,128)(2,1)} %wq.1, bf16[2048,256]{1,0:T(8,128)(2,1)} %wf.1, bf16[2048,256]{1,0:T(8,128)(2,1)} %wi.1, bf16[2048,256]{1,0:T(8,128)(2,1)} %wg.1, bf16[2048,256]{1,0:T(8,128)(2,1)} %wh.1, ...), custom_call_target="tpu_custom_call" | custom-call | tf_op jit(solution)/shard_map/pallas_call | solution.py:720
  36.1 1.0 %copy.18 = bf16[1024,512]{1,0:T(8,128)(2,1)} copy(bf16[1024,512]{1,0:T(8,128)(2,1)S(1)} %shard_map.154) | data formatting | bytes 2097152

commit v5 on v4

--- a/solution.py
+++ b/solution.py
@@ -12,7 +12,7 @@
 ROWS = 256
 MIX_ROWS = 128
 LAG = 2
-EXTRA = 16
+EXTRA = 8
 TAPS = 3
 HALO = 8
 HEAD = 16
@@ -61,7 +61,7 @@
     sent_state, peer_state, sent_total, totals,
     rim, tail, head_conv, head_gate, incoming,
     tok_sem, leak_sem, w_sem, own_sem,
-    pair_send, pair_recv, piece_send, piece_recv, mate_send,
+    pair_send, pair_recv, piece_send, piece_recv, twin_recv, mate_send,
     blk_send, fwd_send, conv_recv, mix_first, mix_recv, l1_send, l1_recv, l2_send, l2_recv, rim_send, rim_recv,
     ready, rim_ready, twin_ready, mate_ready,
 ):
@@ -146,22 +146,26 @@
         return pltpu.make_async_remote_copy(
             outs[kind].at[piece_rows(mine), cols_of(target)],
             columns.at[kind, me, piece_rows(mine)],
-            piece_send.at[kind, k - 1, c], piece_recv.at[kind, chips - k - 1, core, 0],
+            piece_send.at[0], piece_recv.at[kind, chips - k - 1, core, 0],
             device_id={"tp": target},
         )
 
     def piece_in(kind, k, c, n):
-        size = (piece, piece, 2 * piece)[n]
-        ref = columns.at[kind, me, 0:size]
+        ref = columns.at[kind, me, 0:piece]
         return pltpu.make_async_copy(ref, ref, piece_recv.at[kind, k - 1, c, n])
 
     def pass_on(kind, k, c, n):
         g, to = ((mine, mate), (mine, twin), (mates_piece, twin))[n]
         ref = columns.at[kind, far(k, c), piece_rows(g)]
         return pltpu.make_async_remote_copy(
-            ref, ref, mate_send.at[kind, k - 1, c],
-            piece_recv.at[kind, k - 1, c, (1, 2, 2)[n]], device_id={"sp": to},
+            ref, ref, mate_send.at[0],
+            piece_recv.at[kind, k - 1, c, 1] if n == 0 else twin_recv.at[0],
+            device_id={"sp": to},
         )
+
+    def pieces_wait(n, sem):
+        ref = columns.at[:, 0 : tp - 2, 0 : n * piece]
+        pltpu.make_async_copy(ref, ref, sem.at[0]).wait()
 
     def pass_own(kind, wait, which):
         for k, c in far_devices:
@@ -247,13 +251,13 @@
 
     def twin_copy(h):
         return pltpu.make_async_remote_copy(
-            sent_state.at[h], peer_state.at[h], l1_send.at[h], l1_recv.at[h],
+            sent_state.at[h], peer_state.at[h], l1_send.at[0], l1_recv.at[h],
             device_id={"sp": twin},
         )
 
     def total_copy(k, source, h):
         return pltpu.make_async_remote_copy(
-            sent_total.at[h], totals.at[source, h], l2_send.at[h, k - 1], l2_recv.at[h, source],
+            sent_total.at[h], totals.at[source, h], l2_send.at[k - 1], l2_recv.at[source],
             device_id={"sp": lax.rem(place + 2 * k, sp)},
         )
 
@@ -329,6 +333,8 @@
             piece_out(kind, k, c).start()
     for t in range(2, nb):
         token_copy(t).start()
+    for n in (2, 3, 4):
+        weight_copy(n).start()
     for n in (2, 3, 4):
         small_copy(n).start()
     for kind in (CONV, MIX):
@@ -457,7 +463,7 @@
                 decay = jnp.where(member == 0, peer_decay, own_decay)
                 sent_total[h, :GROUP_FEATURES, :] = (early * decay + late).astype(bf16)
                 put_decay(sent_total, h, own_decay * peer_decay)
-                for k in range(1, pairs):
+                for k in reversed(range(1, pairs)):
                     @pl.when(pair + k < pairs)
                     def _():
                         total_copy(k, pair, h).start()
@@ -467,7 +473,7 @@
     norm(0)
     small_copy(1).wait()
     weight_wait(0)
-    for n in range(2, 7):
+    for n in (5, 6):
         weight_copy(n).start()
     product = scan_product(0)
     if nb > 1:
@@ -475,7 +481,7 @@
     for t in range(nb):
         if t + 2 < nb:
             arrive(t + 2)
-        thirds = [n for n in range(3) if t == max(nb - 3 + min(n, 1), 0)]
+        thirds = [n for n in range(3) if t == max(nb - 4 + min(n, 1), 0)]
         for n in thirds:
             weight_copy(2 + n).wait()
         if t + 1 < nb:
@@ -484,7 +490,7 @@
             conv_thirds.append(conv_third(n))
         if t + 2 < nb:
             normalize(t + 2)
-        if t == nb - 1:
+        if t == max(nb - 2, 0):
             for n in (2, 3, 4):
                 small_copy(n).wait()
             conv_block(0, jnp.concatenate(conv_thirds, axis=1))
@@ -584,8 +590,8 @@
     for k in range(1, pairs):
         @pl.when(pair >= k)
         def _():
-            for h in range(heads):
-                total_copy(k, pair - k, h).wait_recv()
+            ref = totals.at[pair - k]
+            pltpu.make_async_copy(ref, ref, l2_recv.at[pair - k]).wait()
     incoming[...] = jnp.zeros_like(incoming)
 
     def hop(p, _):
@@ -640,9 +646,7 @@
 
     relay(CONV, 0)
 
-    for kind in (CONV, MIX):
-        for k, c in far_devices:
-            piece_in(kind, k, c, 2).wait()
+    pieces_wait(2, twin_recv)
     for k in range(1, chips):
         landed(CONV, chips - 1 + k, 0)
 
@@ -658,24 +662,19 @@
 
     sent(CONV)
     passed_on(CONV)
-    for kind in (CONV, MIX):
-        for k, c in far_devices:
-            piece_out(kind, k, c).wait_send()
-            passed = columns.at[kind, me, 0 : 3 * piece]
-            pltpu.make_async_copy(passed, passed, mate_send.at[kind, k - 1, c]).wait()
+    pieces_wait(1, piece_send)
+    pieces_wait(3, mate_send)
     pltpu.make_async_copy(mine_both, mine_both, pair_send.at[0]).wait()
 
     @pl.when(place < sp - 1)
     def _():
         rim_copy.wait_send()
 
-    for h in range(heads):
-        twin_copy(h).wait_send()
+    pltpu.make_async_copy(sent_state, sent_state, l1_send.at[0]).wait()
     for k in range(1, pairs):
         @pl.when(pair + k < pairs)
         def _():
-            for h in range(heads):
-                total_copy(k, pair, h).wait_send()
+            pltpu.make_async_copy(sent_total, sent_total, l2_send.at[k - 1]).wait()
 
     def finish(t, _):
         @pl.when(t + LAG < mix_nb)
@@ -758,11 +757,10 @@
             pltpu.VMEM((HALO, channels), f32),
             pltpu.VMEM(square, f32),
             sems((nb,)), sems((2,)), sems((5,)), sems((1,)),
-            sems((1,)), sems((1,)), sems((2, chips - 1, 2)), sems((2, chips - 1, 2, 3)),
-            sems((2, chips - 1, 2)),
+            sems((1,)), sems((1,)), sems((1,)), sems((2, chips - 1, 2, 2)), sems((1,)), sems((1,)),
             sems((2, chips)), sems((2, chips - 1)), sems((2 * chips - 1,)), sems((1,)),
             sems((2 * chips - 2, count // MIX_ROWS)),
-            sems((heads,)), sems((heads,)), sems((heads, pairs - 1)), sems((heads, pairs)),
+            sems((1,)), sems((heads,)), sems((pairs - 1,)), sems((pairs - 1,)),
             sems((1,)), sems((1,)),
         ] + [pltpu.SemaphoreType.REGULAR] * 4,
         compiler_params=pltpu.CompilerParams(

time: 37.2 us -> 36.4 us (0.978)
  Pallas kernels: 36.1 us -> 35.3 us
    pallas_call x1, Pallas kernels: 36.1 us -> 35.3 us  [body(): pl.pallas_call(functools.partial(fused_kernel, tp, sp, share), in_specs=[...]
where the time goes in v5:
time: 36.4 us; the launch traced here: 36.3 us
  Pallas kernels  35.3 us (97%)
  local copies, waits for them, and re-layouts  0.97 us (3%)
    pallas_call x1, Pallas kernels, body(): pl.pallas_call(functools.partial(fused_kernel, tp, sp, share), in_specs=[...  35.3 us
    unnamed x1, local copies, waits for them, and re-layouts  0.97 us

profile of v5, /device:TPU:1, one launch (start us, length us, event | category | flops | bytes accessed | tf_op | source)
XLA Modules:
  0.0 36.3 jit_solution(13943881322103975998)
XLA Ops:
  0.0 35.3 %shard_map.154 = bf16[1024,512]{1,0:T(8,128)(2,1)S(1)} custom-call(bf16[1024,2048]{1,0:T(8,128)(2,1)} %tokens.1, f32[1,2048]{1,0:T(1,128)} %bitcast.4, bf16[2048,256]{1,0:T(8,128)(2,1)} %wq.1, bf16[2048,256]{1,0:T(8,128)(2,1)} %wf.1, bf16[2048,256]{1,0:T(8,128)(2,1)} %wi.1, bf16[2048,256]{1,0:T(8,128)(2,1)} %wg.1, bf16[2048,256]{1,0:T(8,128)(2,1)} %wh.1, ...), custom_call_target="tpu_custom_call" | custom-call | tf_op jit(solution)/shard_map/pallas_call | solution.py:719
  35.3 1.0 %copy.18 = bf16[1024,512]{1,0:T(8,128)(2,1)} copy(bf16[1024,512]{1,0:T(8,128)(2,1)S(1)} %shard_map.154) | data formatting | bytes 2097152

commit v6 on v5

--- a/solution.py
+++ b/solution.py
@@ -11,7 +11,7 @@
 CHUNK = 128
 ROWS = 256
 MIX_ROWS = 128
-LAG = 2
+LAG = 3
 EXTRA = 8
 TAPS = 3
 HALO = 8

time: 36.4 us -> 36.4 us (level)
  no operation moved by 1% of the time
where the time goes in v6:
time: 36.4 us; the launch traced here: 36.3 us
  Pallas kernels  35.3 us (97%)
  local copies, waits for them, and re-layouts  0.97 us (3%)
    pallas_call x1, Pallas kernels, body(): pl.pallas_call(functools.partial(fused_kernel, tp, sp, share), in_specs=[...  35.3 us
    unnamed x1, local copies, waits for them, and re-layouts  0.97 us

profile of v6, /device:TPU:1, one launch (start us, length us, event | category | flops | bytes accessed | tf_op | source)
XLA Modules:
  0.0 36.3 jit_solution(16066674735516462139)
XLA Ops:
  0.0 35.3 %shard_map.154 = bf16[1024,512]{1,0:T(8,128)(2,1)S(1)} custom-call(bf16[1024,2048]{1,0:T(8,128)(2,1)} %tokens.1, f32[1,2048]{1,0:T(1,128)} %bitcast.4, bf16[2048,256]{1,0:T(8,128)(2,1)} %wq.1, bf16[2048,256]{1,0:T(8,128)(2,1)} %wf.1, bf16[2048,256]{1,0:T(8,128)(2,1)} %wi.1, bf16[2048,256]{1,0:T(8,128)(2,1)} %wg.1, bf16[2048,256]{1,0:T(8,128)(2,1)} %wh.1, ...), custom_call_target="tpu_custom_call" | custom-call | tf_op jit(solution)/shard_map/pallas_call | solution.py:719
  35.3 1.0 %copy.18 = bf16[1024,512]{1,0:T(8,128)(2,1)} copy(bf16[1024,512]{1,0:T(8,128)(2,1)S(1)} %shard_map.154) | data formatting | bytes 2097152
